TPU v7x, 32 devices: a whole 2x2x4 slice. The times are simulated.
32 devices in a mesh: ep: 4 (over y, x), tp: 8 (over z, core).
Axes of the slice: x: 2, y: 2, z: 4, core: 2. Of those that a mesh axis runs over, the one named last changes fastest.
Arguments:
- tokens: bfloat16 [256, 4096], P('ep'), may hold values from -6 to 6
- norm_gain: float32 [4096], replicated, may hold values from 0.1 to 1.9
- ffn_gain: float32 [4096], replicated, may hold values from 0.1 to 1.9
- w_in: bfloat16 [4096, 2048], P(None, 'tp'), may hold values from -0.09375 to 0.09375
- decay_rate: float32 [8192], P('tp'), may hold values from 0.02 to 2
- frequency: float32 [8192], P('tp'), may hold values from -3.140625 to 3.140625
- log_step: float32 [128], P('tp'), may hold values from -2.3 to 0
- input_real: float32 [16, 8192], P(None, 'tp'), may hold values from -1 to 1
- input_imag: float32 [16, 8192], P(None, 'tp'), may hold values from -1 to 1
- readout_real: float32 [16, 8192], P(None, 'tp'), may hold values from -0.5 to 0.5
- readout_imag: float32 [16, 8192], P(None, 'tp'), may hold values from -0.5 to 0.5
- skip_gain: float32 [2048], P('tp'), may hold values from -4 to 4
- state_real: float32 [256, 8192], P('ep', 'tp'), may hold values from -6 to 6
- state_imag: float32 [256, 8192], P('ep', 'tp'), may hold values from -6 to 6
- w_out: bfloat16 [2048, 4096], P('tp'), may hold values from -0.125 to 0.125
- shared_gate: bfloat16 [4096, 1024], P(None, 'tp'), may hold values from -0.09375 to 0.09375
- shared_up: bfloat16 [4096, 1024], P(None, 'tp'), may hold values from -0.09375 to 0.09375
- shared_down: bfloat16 [1024, 4096], P('tp'), may hold values from -0.1875 to 0.1875
- expert_gate: bfloat16 [16, 4096, 1024], P('ep', 'tp'), may hold values from -0.09375 to 0.09375
- expert_up: bfloat16 [16, 4096, 1024], P('ep', 'tp'), may hold values from -0.09375 to 0.09375
- expert_down: bfloat16 [16, 1024, 4096], P('ep', None, 'tp'), may hold values from -0.1875 to 0.1875
- routing: int32 [256, 4], P('ep'), may hold values from 0 to 15, all different within a row; in each aligned block of 64 rows (0 to 63, 64 to 127, ...) at most 32 rows name the same one
- route_weight: float32 [256, 4], P('ep'), may hold values from 0.1 to 1
Outputs:
- mixed: bfloat16 [256, 4096], P('ep', 'tp')
- new_state_real: float32 [256, 8192], P('ep', 'tp')
- new_state_imag: float32 [256, 8192], P('ep', 'tp')
Inputs may be any that keep to these rules, and one draw needn't show every extreme that they name: `routing`: each row names 4 different experts. In the rows of one index of ep (aligned blocks of 64 rows) no expert is named more than 32 times, and in every draw some expert is named exactly 32 times in some block.
All inputs are finite; a program needn't handle non-finite values.
Results may differ from a plain program's by a relative error of at most 0.02.
Values may be sent and summed in bfloat16 or wider, within the bound.
No kernel may reach another device: no remote copies, remote signals or barrier semaphores. Data moves between devices by JAX's collectives and lax.ppermute only.
A program may use at most 64 MiB of HBM per device.

v0:
```python
import jax
import jax.numpy as jnp
from jax import lax
from jax.sharding import PartitionSpec as P

EPS = 1e-06
ROUTED_SCALE = 2.5
HIGH = lax.Precision.HIGHEST


def rms_scale(values_in, gains):
    values = values_in.astype(jnp.float32)
    factor = lax.rsqrt(jnp.mean(values * values, axis=-1, keepdims=True) + EPS)
    return (values * factor * gains).astype(jnp.bfloat16)


def state_update(
    normed,
    w_in,
    decay_rate,
    frequency,
    log_step,
    input_real,
    input_imag,
    readout_real,
    readout_imag,
    skip_gain,
    state_real,
    state_imag,
):
    seq_count = normed.shape[0]
    groups = log_step.shape[0]
    chan_count = skip_gain.shape[0] // groups
    state_width = decay_rate.shape[0] // groups
    drive_rows = jnp.dot(normed, w_in, preferred_element_type=jnp.float32).astype(jnp.bfloat16)
    drive_f = drive_rows.astype(jnp.float32).reshape(seq_count, groups, chan_count)
    decays = decay_rate.reshape(groups, state_width)
    omegas = frequency.reshape(groups, state_width)
    step_size = jnp.exp(log_step)[:, None]
    pole_mag = jnp.exp(-decays * step_size)
    pole_angle = omegas * step_size
    pole_re = pole_mag * jnp.cos(pole_angle)
    pole_im = pole_mag * jnp.sin(pole_angle)
    pole_norm = decays * decays + omegas * omegas
    diff_re = pole_re - 1.0
    lift_re = (-decays * diff_re + omegas * pole_im) / pole_norm
    lift_im = (-decays * pole_im - omegas * diff_re) / pole_norm
    in_re = input_real.reshape(chan_count, groups, state_width)
    in_im = input_imag.reshape(chan_count, groups, state_width)
    push_re = jnp.einsum("sgh,hgp->sgp", drive_f, in_re, precision=HIGH)
    push_im = jnp.einsum("sgh,hgp->sgp", drive_f, in_im, precision=HIGH)
    old_re = state_real.reshape(seq_count, groups, state_width)
    old_im = state_imag.reshape(seq_count, groups, state_width)
    new_re = pole_re * old_re - pole_im * old_im + lift_re * push_re - lift_im * push_im
    new_im = pole_re * old_im + pole_im * old_re + lift_re * push_im + lift_im * push_re
    out_re = readout_real.reshape(chan_count, groups, state_width)
    out_im = readout_imag.reshape(chan_count, groups, state_width)
    read_rows = jnp.einsum("sgp,hgp->sgh", new_re, out_re, precision=HIGH) - jnp.einsum(
        "sgp,hgp->sgh", new_im, out_im, precision=HIGH
    )
    read_rows = read_rows + skip_gain.reshape(groups, chan_count) * drive_f
    activated = jax.nn.gelu(read_rows).reshape(seq_count, groups * chan_count).astype(jnp.bfloat16)
    return (
        activated,
        new_re.reshape(seq_count, groups * state_width),
        new_im.reshape(seq_count, groups * state_width),
    )


def local(
    tokens,
    norm_gain,
    ffn_gain,
    w_in,
    decay_rate,
    frequency,
    log_step,
    input_real,
    input_imag,
    readout_real,
    readout_imag,
    skip_gain,
    state_real,
    state_imag,
    w_out,
    shared_gate,
    shared_up,
    shared_down,
    expert_gate,
    expert_up,
    expert_down,
    routing,
    route_weight,
):
    seq_count, model_width = tokens.shape
    tp_count = lax.axis_size("tp")
    ep_count = lax.axis_size("ep")
    slice_width = model_width // tp_count
    offset = lax.axis_index("tp") * slice_width
    normed = rms_scale(tokens, norm_gain)
    activated, new_real, new_imag = state_update(
        normed,
        w_in,
        decay_rate,
        frequency,
        log_step,
        input_real,
        input_imag,
        readout_real,
        readout_imag,
        skip_gain,
        state_real,
        state_imag,
    )
    mixer_terms = jnp.dot(activated, w_out, preferred_element_type=jnp.float32)
    mixer_own = lax.psum_scatter(mixer_terms, "tp", scatter_dimension=1, tiled=True)
    own_tokens = lax.dynamic_slice_in_dim(tokens, offset, slice_width, 1)
    resid_own = (own_tokens.astype(jnp.float32) + mixer_own).astype(jnp.bfloat16)
    resid_f = resid_own.astype(jnp.float32)
    square_sum = lax.psum(jnp.sum(resid_f * resid_f, axis=1, keepdims=True), "tp")
    factor = lax.rsqrt(square_sum / model_width + EPS)
    gain_own = lax.dynamic_slice_in_dim(ffn_gain, offset, slice_width, 0)
    rows_own = (resid_f * factor * gain_own).astype(jnp.bfloat16)
    ffn_rows = lax.all_gather(rows_own, "tp", axis=1, tiled=True)
    expert_dev = expert_gate.shape[0]
    expert_count = expert_dev * ep_count
    top_count = routing.shape[1]
    capacity = 2 * seq_count * top_count // expert_count
    slot_count = expert_count * capacity
    flat_ids = routing.reshape(-1)
    one_hot = (flat_ids[:, None] == jnp.arange(expert_count, dtype=jnp.int32)[None, :]).astype(
        jnp.int32
    )
    earlier = jnp.cumsum(one_hot, axis=0) - one_hot
    slot_rank = jnp.sum(earlier * one_hot, axis=1)
    target = flat_ids * capacity + slot_rank
    slot_ids = jnp.arange(slot_count, dtype=jnp.int32)
    placed = (target[None, :] == slot_ids[:, None]).reshape(slot_count, seq_count, top_count)
    dispatch_map = jnp.sum(placed.astype(jnp.float32), axis=2).astype(jnp.bfloat16)
    outgoing = jnp.dot(dispatch_map, rows_own, preferred_element_type=jnp.float32).astype(
        jnp.bfloat16
    )
    outgoing = outgoing.reshape(ep_count, expert_dev * capacity, slice_width)
    incoming = lax.all_to_all(outgoing, "ep", split_axis=0, concat_axis=0, tiled=True)
    arrived = incoming.reshape(ep_count, expert_dev, capacity, slice_width)
    gate_part = jnp.einsum(
        "secd,edf->secf", arrived, expert_gate, preferred_element_type=jnp.float32
    )
    up_part = jnp.einsum("secd,edf->secf", arrived, expert_up, preferred_element_type=jnp.float32)
    gate_full, up_full = (
        lax.psum(gate_part.astype(jnp.bfloat16), "tp").astype(jnp.float32),
        lax.psum(up_part.astype(jnp.bfloat16), "tp").astype(jnp.float32),
    )
    inner_rows = (jax.nn.silu(gate_full) * up_full).astype(jnp.bfloat16)
    expert_terms = jnp.einsum(
        "secf,efd->secd", inner_rows, expert_down, preferred_element_type=jnp.float32
    )
    returned = lax.all_to_all(
        expert_terms.reshape(ep_count, expert_dev * capacity, slice_width).astype(jnp.bfloat16),
        "ep",
        split_axis=0,
        concat_axis=0,
        tiled=True,
    ).astype(jnp.float32)
    weights = route_weight / jnp.sum(route_weight, axis=1, keepdims=True) * ROUTED_SCALE
    chosen = target.reshape(seq_count, top_count)[:, :, None] == slot_ids[None, None, :]
    combine = jnp.sum(jnp.where(chosen, weights[:, :, None], 0.0), axis=1)
    routed = jnp.dot(combine, returned.reshape(slot_count, slice_width), precision=HIGH)
    shared_gate_rows = jnp.dot(ffn_rows, shared_gate, preferred_element_type=jnp.float32)
    shared_up_rows = jnp.dot(ffn_rows, shared_up, preferred_element_type=jnp.float32)
    shared_inner = (jax.nn.silu(shared_gate_rows) * shared_up_rows).astype(jnp.bfloat16)
    shared_terms = jnp.dot(shared_inner, shared_down, preferred_element_type=jnp.float32)
    shared_own = lax.psum_scatter(
        shared_terms.astype(jnp.bfloat16), "tp", scatter_dimension=1, tiled=True
    ).astype(jnp.float32)
    mixed = (resid_own.astype(jnp.float32) + shared_own + routed).astype(jnp.bfloat16)
    return (mixed, new_real, new_imag)


def solution(mesh):
    placed = (
        P("ep", None),
        P(),
        P(),
        P(None, "tp"),
        P("tp"),
        P("tp"),
        P("tp"),
        P(None, "tp"),
        P(None, "tp"),
        P(None, "tp"),
        P(None, "tp"),
        P("tp"),
        P("ep", "tp"),
        P("ep", "tp"),
        P("tp", None),
        P(None, "tp"),
        P(None, "tp"),
        P("tp", None),
        P("ep", "tp", None),
        P("ep", "tp", None),
        P("ep", None, "tp"),
        P("ep", None),
        P("ep", None),
    )
    return jax.shard_map(
        local,
        mesh=mesh,
        in_specs=placed,
        out_specs=(P("ep", "tp"), P("ep", "tp"), P("ep", "tp")),
        check_vma=False,
    )
```

profile of v0, /device:TPU:0, one launch (start us, length us, event | category | flops | bytes accessed | tf_op | source)
XLA Modules:
  0.0 197.0 jit_solution(18267901409263895610)
XLA Ops:
  8.1 1.2 fusion.34
  11.7 2.3 %convolution_convert_fusion.2 = bf16[64,256]{1,0:T(8,128)(2,1)S(1)} fusion(bf16[4096,256]{1,0:T(8,128)(2,1)} %param.26, bf16[64,4096]{1,0:T(8,128)(2,1)} %param.23, f32[4096]{0:T(1024)} %param.24, f32[64]{0:T(128)S(1)} %add_rsqrt_fusion), kind=kOutput, calls=%fused_computation.28 | convolution fusion | flops 135282688 | bytes 2670848 | tf_op jit(solution)/shard_map/dot_general | solution.py:35
  15.2 1.0 reshape.246
  16.1 0.9 reshape.247
  17.6 1.9 bitcast_add_fusion
  19.6 0.9 fusion.55
  20.5 1.0 fusion.50
  21.5 1.5 fusion.75
  25.5 33.1 %reduce-scatter.3.cloned.1.call-done = f32[64,512]{1,0:T(8,128)} async-done(((f32[64,4096]{1,0:T(8,128)}), f32[64,512]{1,0:T(8,128)}) %reduce-scatter.3.cloned.1.call-update) | async-done | bytes 131088 | tf_op jit(solution)/shard_map/reduce_scatter | solution.py:116
  58.5 1.0 fusion.51
  59.6 13.9 %psum.21 = f32[64,1]{0,1:T(1,128)S(1)} all-reduce(f32[64,1]{0,1:T(1,128)S(1)} %bitcast.105), channel_id=1, replica_groups=mesh['ep'=4,'tp'=8] {'tp'}, use_global_device_ids=true, to_apply=%region_3.0 | all-reduce | flops 64 | bytes 512 | tf_op jit(solution)/shard_map/psum | solution.py:120
  73.9 11.7 %all_to_all.10 = bf16[4,128,512]{2,1,0:T(8,128)(2,1)S(1)} all-to-all(bf16[4,128,512]{2,1,0:T(8,128)(2,1)S(1)} %bitcast.99), channel_id=1, replica_groups=mesh['ep'=4,'tp'=8] {'ep'}, dimensions={0} | all-to-all | bytes 1048576 | tf_op jit(solution)/shard_map/all_to_all | solution.py:144
  85.6 4.0 %fusion.17 = bf16[4,4,32,1024]{3,2,0,1:T(8,128)(2,1)} fusion(bf16[4,512,1024]{2,1,0:T(8,128)(2,1)} %param.42, bf16[4,4,32,512]{3,2,1,0:T(8,128)(2,1)S(1)} %bitcast.97), kind=kOutput, calls=%fused_computation.16 | convolution fusion | flops 537395200 | bytes 5767168 | tf_op jit(solution)/shard_map/secd,edf->secf/dot_general | solution.py:149
  89.6 1.7 fusion.20
  91.4 16.5 %all_gather.3 = bf16[64,4096]{1,0:T(8,128)(2,1)S(1)} all-gather(bf16[64,512]{1,0:T(8,128)(2,1)S(1)} %fusion.53), channel_id=1, replica_groups=mesh['ep'=4,'tp'=8] {'tp'}, dimensions={1}, use_global_device_ids=true | all-gather | bytes 589824 | tf_op jit(solution)/shard_map/all_gather | solution.py:124
  107.9 1.5 fusion.76
  109.5 3.0 %convolution_convert_fusion = bf16[64,4096]{1,0:T(8,128)(2,1)} fusion(bf16[128,4096]{1,0:T(8,128)(2,1)} %param.40, bf16[64,4096]{1,0:T(8,128)(2,1)S(1)} %all_gather.3, bf16[4096,128]{1,0:T(8,128)(2,1)} %param.39, f32[64,128]{1,0:T(8,128)S(1)} %fusion.76), kind=kOutput, calls=%fused_computation | convolution fusion | flops 134529024 | bytes 3178496 | tf_op jit(solution)/shard_map/dot_general | solution.py:172
  112.5 42.7 %all-reduce.3.cloned.1.call-done = (bf16[4,4,32,1024]{3,2,0,1:T(8,128)(2,1)}, bf16[4,4,32,1024]{3,2,0,1:T(8,128)(2,1)}) async-done(((bf16[4,4,32,1024]{3,2,0,1:T(8,128)(2,1)}, bf16[4,4,32,1024]{3,2,0,1:T(8,128)(2,1)}), (bf16[4,4,32,1024]{3,2,0,1:T(8,128)(2,1)}, bf16[4,4,32,1024]{3,2,0,1:T(8,128)(2,1)})) %all-reduce.3.cloned.1.call-update) | async-done | bytes 2097168 | tf_op jit(solution)/shard_map/psum | solution.py:152
  155.1 3.7 %fusion.26 = bf16[4,4,32,512]{3,2,0,1:T(8,128)(2,1)S(1)} fusion(bf16[4,1024,512]{2,1,0:T(8,128)(2,1)} %param.43, bf16[4,4,32,1024]{3,2,0,1:T(8,128)(2,1)} %get-tuple-element.3, bf16[4,4,32,1024]{3,2,0,1:T(8,128)(2,1)} %get-tuple-element.4), kind=kOutput, calls=%fused_computation.22 | convolution fusion | flops 541327360 | bytes 6815744 | tf_op jit(solution)/shard_map/secf,efd->secd/dot_general | solution.py:155
  159.7 4.1 %all-to-all-start.1 = ((bf16[4,128,512]{2,1,0:T(8,128)(2,1)}), bf16[4,128,512]{2,1,0:T(8,128)(2,1)}, u32[]{:S(2)}, u32[]{:S(2)}) async-start(bf16[4,128,512]{2,1,0:T(8,128)(2,1)} %bitcast.100), calls=%async_computation.3 | async-start | bytes 1048576 | tf_op jit(solution)/shard_map/all_to_all | solution.py:158
  163.9 1.1 copy.93
  165.3 1.9 reshape.259
  168.3 20.2 %reduce-scatter.5.cloned.1.call-done = bf16[64,512]{1,0:T(8,128)(2,1)} async-done(((bf16[64,4096]{1,0:T(8,128)(2,1)}), bf16[64,512]{1,0:T(8,128)(2,1)}) %reduce-scatter.5.cloned.1.call-update) | async-done | bytes 65552 | tf_op jit(solution)/shard_map/reduce_scatter | solution.py:173
  188.4 2.1 %fusion.31 = bf16[64,512]{1,0:T(8,128)(2,1)} fusion(f32[64,512]{1,0:T(8,128)S(1)} %select_reduce_fusion, bf16[512,512]{1,0:T(8,128)(2,1)} %bitcast.22, bf16[64,512]{1,0:T(8,128)(2,1)S(1)} %get-tuple-element.6, bf16[64,512]{1,0:T(8,128)(2,1)} %reduce-scatter.5.cloned.1.call-done), kind=kOutput, calls=%fused_computation.27 | convolution fusion | flops 201490432 | bytes 851968 | tf_op jit(solution)/shard_map/dot_general | solution.py:168
  (70 shorter events, 10.0 us)
Async XLA Ops:
  7.2 14.4 %copy-start = (bf16[256,4096]{1,0:T(8,128)(2,1)S(1)}, bf16[256,4096]{1,0:T(8,128)(2,1)}, u32[]{:S(2)}) copy-start(bf16[256,4096]{1,0:T(8,128)(2,1)} %param.37) | copy-start | bytes 6291460
  7.2 7.0 %copy-start.7 = (f32[16,1024]{1,0:T(8,128)S(1)}, f32[16,1024]{1,0:T(8,128)}, u32[]{:S(2)}) copy-start(f32[16,1024]{1,0:T(8,128)} %param.30) | copy-start | bytes 196612
  7.2 7.1 %copy-start.8 = (f32[16,1024]{1,0:T(8,128)S(1)}, f32[16,1024]{1,0:T(8,128)}, u32[]{:S(2)}) copy-start(f32[16,1024]{1,0:T(8,128)} %param.31) | copy-start | bytes 196612
  7.2 7.2 %copy-start.9 = (f32[16,1024]{1,0:T(8,128)S(1)}, f32[16,1024]{1,0:T(8,128)}, u32[]{:S(2)}) copy-start(f32[16,1024]{1,0:T(8,128)} %param.32) | copy-start | bytes 196612
  7.2 7.9 %copy-start.10 = (f32[16,1024]{1,0:T(8,128)S(1)}, f32[16,1024]{1,0:T(8,128)}, u32[]{:S(2)}) copy-start(f32[16,1024]{1,0:T(8,128)} %param.33) | copy-start | bytes 196612
  7.2 8.0 %copy-start.5 = (f32[64,1024]{1,0:T(8,128)S(1)}, f32[64,1024]{1,0:T(8,128)}, u32[]{:S(2)}) copy-start(f32[64,1024]{1,0:T(8,128)} %param.35) | copy-start | bytes 786436
  7.2 51.3 %reduce-scatter.3.cloned.1.call-start = ((), (), s32[]{:S(2)}) async-start(), calls=%async_computation.4 | async-start | bytes 1179648 | tf_op jit(solution)/shard_map/reduce_scatter | solution.py:116
  11.7 4.4 %copy-start.6 = (f32[64,1024]{1,0:T(8,128)S(1)}, f32[64,1024]{1,0:T(8,128)}, u32[]{:S(2)}) copy-start(f32[64,1024]{1,0:T(8,128)} %param.36) | copy-start | bytes 786436
  17.1 2.5 %copy-start.4 = (f32[16,16,64]{2,1,0:T(8,128)S(1)}, f32[16,16,64]{2,1,0:T(8,128)}, u32[]{:S(2)}) copy-start(f32[16,16,64]{2,1,0:T(8,128)} %reshape.251) | copy-start | bytes 196612
  19.6 3.5 %copy-start.1 = (f32[64,16,64]{2,0,1:T(8,128)}, f32[64,16,64]{2,0,1:T(8,128)S(1)}, u32[]{:S(2)}) copy-start(f32[64,16,64]{2,0,1:T(8,128)S(1)} %get-tuple-element.7) | copy-start | bytes 786436
  21.5 1.6 copy-start.11
  23.1 132.1 %all-reduce.3.cloned.1.call-start = ((), (), s32[]{:S(2)}) async-start(), calls=%async_computation.6 | async-start | bytes 4194304 | tf_op jit(solution)/shard_map/psum | solution.py:152
  85.6 4.0 %copy-start.3 = (bf16[4,512,1024]{2,1,0:T(8,128)(2,1)S(1)}, bf16[4,512,1024]{2,1,0:T(8,128)(2,1)}, u32[]{:S(2)}) copy-start(bf16[4,512,1024]{2,1,0:T(8,128)(2,1)} %param.41) | copy-start | bytes 12582916
  91.4 97.0 %reduce-scatter.5.cloned.1.call-start = ((), (), s32[]{:S(2)}) async-start(), calls=%async_computation.5 | async-start | bytes 589824 | tf_op jit(solution)/shard_map/reduce_scatter | solution.py:173
  158.8 5.0 %copy-start.2 = (f32[64,16,64]{2,0,1:T(8,128)S(1)}, f32[64,16,64]{2,0,1:T(8,128)}, u32[]{:S(2)}) copy-start(f32[64,16,64]{2,0,1:T(8,128)} %copy-done.1) | copy-start | bytes 786436
  159.7 28.7 %all-to-all-start.1 = ((bf16[4,128,512]{2,1,0:T(8,128)(2,1)}), bf16[4,128,512]{2,1,0:T(8,128)(2,1)}, u32[]{:S(2)}, u32[]{:S(2)}) async-start(bf16[4,128,512]{2,1,0:T(8,128)(2,1)} %bitcast.100), calls=%async_computation.3 | async-start | bytes 1048576 | tf_op jit(solution)/shard_map/all_to_all | solution.py:158
  163.9 4.2 %copy-start.12 = (f32[64,4]{0,1:T(4,128)S(1)}, f32[64,4]{0,1:T(4,128)}, u32[]{:S(2)}) copy-start(f32[64,4]{0,1:T(4,128)} %param.45) | copy-start | bytes 3076
Sparse Core Ops, SparseCore 0:
  23.2 35.2 reduce-scatter.2
  91.5 63.6 all-reduce.2
  157.4 30.9 reduce-scatter.4
where the time goes:
time: 198 us; the launch traced here: 197 us
  waiting for transfers between devices  96 us (48%)
  blocking collectives  42.1 us (21%)
  matrix products  24.4 us (12%)
  between operations  14 us (7%)
  local copies, waits for them, and re-layouts  12 us (6%)
  starting transfers between devices  4.25 us (2%)
  other arithmetic  4.21 us (2%)
    psum x1, waiting for transfers between devices, local(): lax.psum(up_part.astype(jnp.bfloat16), 'tp').astype(jnp.float32)  42.7 us
    reduce_scatter x1, waiting for transfers between devices, local(): lax.psum_scatter(mixer_terms, 'tp', scatter_dimension=1, tiled=True)  33.1 us
    reduce_scatter x1, waiting for transfers between devices, local(): lax.psum_scatter(shared_terms.astype(jnp.bfloat16), 'tp', scatter_dimensi...  20.2 us
    all_gather x1, blocking collectives, local(): ffn_rows = lax.all_gather(rows_own, 'tp', axis=1, tiled=True)  16.5 us
    psum x1, blocking collectives, local(): lax.psum(jnp.sum(resid_f * resid_f, axis=1, keepdims=True), 'tp')  13.9 us
    all_to_all x1, blocking collectives, local(): lax.all_to_all(outgoing, 'ep', split_axis=0, concat_axis=0, tiled=True)  11.7 us
    all_to_all x1, starting transfers between devices, local(): lax.all_to_all(expert_terms.reshape(ep_count, expert_dev * capacity, slic...  4.13 us
    dot_general x1, matrix products, local(): jnp.einsum('secd,edf->secf', arrived, expert_up, preferred_element_type=j...  4.04 us
  transfers between devices with their start and end apart: 4, of which 3 were waited for; matrix products, arithmetic and copies ran while one was open for 8% of the time, Pallas kernels for 0%

commit v1 on v0

v1 whole, which is shorter than its diff:
```python
import functools

import jax
import jax.numpy as jnp
from jax import lax
from jax.experimental import pallas as pl
from jax.experimental.pallas import tpu as pltpu
from jax.sharding import PartitionSpec as P


EPS = 1e-06
ROUTED_SCALE = 2.5
LANES = 128
MIB = 1 << 20
HIGH = lax.Precision.HIGHEST
F32 = jnp.float32
BF16 = jnp.bfloat16
IN_VMEM = pl.BlockSpec(memory_space=pltpu.VMEM)
IN_SMEM = pl.BlockSpec(memory_space=pltpu.SMEM)
IN_HBM = pl.BlockSpec(memory_space=pltpu.HBM)


def in_hbm(*arrays):
    return [pltpu.with_memory_space_constraint(x, pltpu.HBM) for x in arrays]


def dot(a, b, **kwargs):
    return jnp.dot(a, b, preferred_element_type=F32, **kwargs)


def partner(index, step, size):
    return index ^ step if size & (size - 1) == 0 else (index + step) % size


def back(index, step, size):
    return index ^ step if size & (size - 1) == 0 else (index - step) % size


def tp_layout():
    size = lax.axis_size("tp")
    return size // 2, [(i, i ^ 1) for i in range(size)]


def send_line(blocks):
    chips = tp_layout()[0]
    got = [blocks[0]]
    for step in range(1, chips):
        pairs = [
            (2 * z + c, 2 * partner(z, step, chips) + c) for z in range(chips) for c in range(2)
        ]
        got.append(lax.ppermute(blocks[step], "tp", pairs))
    return got


def send_ep(blocks):
    size = lax.axis_size("ep")
    got = [blocks[0]]
    for step in range(1, size):
        pairs = [(i, partner(i, step, size)) for i in range(size)]
        got.append(lax.ppermute(blocks[step], "ep", pairs))
    return got


def pair_sum(keep, give):
    chips, swap = tp_layout()
    got = lax.ppermute(give, "tp", swap)
    return [(keep[j] + got[j].astype(F32)).astype(BF16) for j in range(chips)]


def line_gather(block):
    chips, swap = tp_layout()
    mine = send_line([block] * chips)
    return mine, [lax.ppermute(b, "tp", swap) for b in mine]


def total_of(blocks):
    out = blocks[0].astype(F32)
    for block in blocks[1:]:
        out = out + block.astype(F32)
    return out


def call(kernel, out_shape, in_specs, scratch=(), limit=24):
    specs = jax.tree.map(lambda leaf: IN_VMEM, out_shape)
    return pl.pallas_call(
        kernel,
        out_shape=out_shape,
        in_specs=in_specs,
        out_specs=specs,
        scratch_shapes=list(scratch),
        compiler_params=pltpu.CompilerParams(vmem_limit_bytes=limit * MIB),
    )


def column_block(ref, index, width):
    return ref[:, pl.ds(pl.multiple_of(index * width, width), width)]


def load_all(sources, targets, sems):
    copies = [
        pltpu.make_async_copy(a, b, sems.at[i]) for i, (a, b) in enumerate(zip(sources, targets))
    ]
    for copy in copies:
        copy.start()
    return copies


def state_kernel(chips, spot_ref, log_step, *refs):
    sources, (keep, give, new_re, new_im) = refs[:13], refs[13:17]
    targets, acts, sems = refs[17:30], refs[30], refs[31]
    (
        tokens, gain, w_in, decay, omega, in_re, in_im, old_re, old_im, read_re, read_im, skip, w_out
    ) = targets
    copies = load_all(sources, targets, sems)
    copies[0].wait()
    copies[1].wait()
    groups = log_step.shape[0]
    chan_count = in_re.shape[0]
    channels, states = skip.shape[1], decay.shape[1]
    width = states // groups
    values = tokens[...].astype(F32)
    factor = lax.rsqrt(jnp.mean(values * values, axis=1, keepdims=True) + EPS)
    normed = (values * factor * gain[...]).astype(BF16)

    group_of = lax.broadcasted_iota(jnp.int32, (1, states), 1) // width
    step = jnp.zeros((1, states), F32)
    for g in range(groups):
        step = jnp.where(group_of == g, log_step[g], step)
    step = jnp.exp(step)
    copies[3].wait()
    copies[4].wait()
    decays, omegas = decay[...], omega[...]
    size = jnp.exp(-decays * step)
    angle = omegas * step
    pole_re, pole_im = size * jnp.cos(angle), size * jnp.sin(angle)
    norm = decays * decays + omegas * omegas
    diff = pole_re - 1.0
    lift_re = (-decays * diff + omegas * pole_im) / norm
    lift_im = (-decays * pole_im - omegas * diff) / norm

    copies[2].wait()
    for copy in copies[5:12]:
        copy.wait()
    drive = dot(normed, w_in[...]).astype(BF16).astype(F32)
    block = min(channels, LANES)
    span = block // chan_count * width
    row = lax.broadcasted_iota(jnp.int32, (block, span), 0) // chan_count
    col = lax.broadcasted_iota(jnp.int32, (block, span), 1) // width
    same = row == col

    def spread(ref, at):
        part = ref[:, at : at + span]
        return jnp.where(same, jnp.concatenate([part] * (block // chan_count), axis=0), 0.0)

    for b in range(channels // block):
        at = b * span
        here = slice(at, at + span)
        part = drive[:, b * block : (b + 1) * block]
        push_re = dot(part, spread(in_re, at), precision=HIGH)
        push_im = dot(part, spread(in_im, at), precision=HIGH)
        was_re, was_im = old_re[:, here], old_im[:, here]
        p_re, p_im, l_re, l_im = pole_re[:, here], pole_im[:, here], lift_re[:, here], lift_im[:, here]
        now_re = p_re * was_re - p_im * was_im + l_re * push_re - l_im * push_im
        now_im = p_re * was_im + p_im * was_re + l_re * push_im + l_im * push_re
        new_re[:, here] = now_re
        new_im[:, here] = now_im
        across = (((1,), (1,)), ((), ()))
        read = lax.dot_general(
            now_re, spread(read_re, at), across, precision=HIGH, preferred_element_type=F32
        ) - lax.dot_general(
            now_im, spread(read_im, at), across, precision=HIGH, preferred_element_type=F32
        )
        read = read + skip[:, b * block : (b + 1) * block] * part
        acts[:, b * block : (b + 1) * block] = jax.nn.gelu(read).astype(BF16)
    copies[12].wait()
    emit_columns(chips, spot_ref, acts[...], w_out, keep, give)


def emit_columns(chips, spot_ref, rows, weights, keep, give):
    side, chip = spot_ref[0], spot_ref[2]
    slice_width = keep.shape[2]
    for j in range(chips):
        to = 2 * partner(chip, j, chips)
        keep[j] = dot(rows, column_block(weights, to + side, slice_width))
        give[j] = dot(rows, column_block(weights, to + 1 - side, slice_width)).astype(BF16)


def shared_kernel(chips, spot_ref, gain, *refs):
    side, chip = spot_ref[0], spot_ref[2]
    mine, other, sources = refs[:chips], refs[chips : 2 * chips], refs[2 * chips : 2 * chips + 3]
    keep, give = refs[2 * chips + 3 : 2 * chips + 5]
    gate, up, down, sems = refs[2 * chips + 5 :]
    copies = load_all(sources, (gate, up, down), sems)
    seq_count, slice_width = mine[0].shape
    total = jnp.zeros((seq_count, 1), F32)
    for part in mine + other:
        values = part[...].astype(F32)
        total = total + jnp.sum(values * values, axis=1, keepdims=True)
    factor = lax.rsqrt(total / (2 * chips * slice_width) + EPS)
    gate_rows = jnp.zeros((seq_count, gate.shape[1]), F32)
    up_rows = gate_rows
    copies[0].wait()
    copies[1].wait()
    for j in range(chips):
        source = 2 * back(chip, j, chips)
        for part, index in ((mine[j], source + side), (other[j], source + 1 - side)):
            scaled = part[...].astype(F32) * factor * column_block(gain, index, slice_width)
            rows = scaled.astype(BF16)
            here = pl.ds(pl.multiple_of(index * slice_width, slice_width), slice_width)
            gate_rows = gate_rows + dot(rows, gate[here, :])
            up_rows = up_rows + dot(rows, up[here, :])
    inner = (jax.nn.silu(gate_rows) * up_rows).astype(BF16)
    copies[2].wait()
    emit_columns(chips, spot_ref, inner, down, keep, give)


def placement(spot_ref, code, expert_dev, expert_count):
    first = spot_ref[1]
    token_count, lanes = code.shape
    row = lax.broadcasted_iota(jnp.int32, (8, lanes), 0)
    col = lax.broadcasted_iota(jnp.int32, (8, lanes), 1)
    pick = (row < expert_dev) & ((col == first + row) | (col == first + row + expert_count))
    across = (((1,), (1,)), ((), ()))
    weights = lax.dot_general(
        pick.astype(F32).astype(BF16), code, across, preferred_element_type=F32
    )
    taken = (weights > 0).astype(F32)
    square = (token_count, token_count)
    earlier = lax.broadcasted_iota(jnp.int32, square, 0) < lax.broadcasted_iota(jnp.int32, square, 1)
    before = dot(taken.astype(BF16), earlier.astype(F32).astype(BF16))
    loads = jnp.sum(taken, axis=1, keepdims=True)
    starts, so_far = [], jnp.zeros((1, 1), F32)
    for e in range(expert_dev):
        starts.append(so_far)
        so_far = so_far + loads[e : e + 1]
    starts.append(so_far)
    return weights, taken, before, starts


def expert_kernel(chips, ep_count, expert_count, spot_ref, gain, *refs):
    parts, (gate_hbm, up_hbm) = refs[:ep_count], refs[ep_count : ep_count + 2]
    keep, give, gate, up, message, scaled, acc, sems = refs[ep_count + 2 :]
    expert_dev, slice_width, hidden = gate.shape
    copies = [
        load_all((gate_hbm.at[e], up_hbm.at[e]), (gate.at[e], up.at[e]), sems.at[e])
        for e in range(expert_dev)
    ]
    side, chip = spot_ref[0], spot_ref[2]
    slots = acc.shape[0]
    share = slots // (2 * chips)
    rows = parts[0].shape[0]
    for j in range(ep_count):
        message[j * rows : (j + 1) * rows] = parts[j][...]
    token_count = message.shape[0]
    code = message[:, slice_width:]
    _, taken, before, starts = placement(spot_ref, code, expert_dev, expert_count)
    slot = lax.broadcasted_iota(jnp.int32, (slots, token_count), 0).astype(F32)
    hit = jnp.zeros((slots, token_count), F32)
    for e in range(expert_dev):
        place = jnp.where(taken[e : e + 1] > 0, before[e : e + 1] + starts[e], -1.0)
        hit = hit + (slot == place).astype(F32)
    picked = dot(hit.astype(BF16), message[:, :slice_width])
    squares = picked * picked
    lanes = squares[:, :LANES]
    for at in range(LANES, slice_width, LANES):
        lanes = lanes + squares[:, at : at + LANES]
    scaled[...] = (picked * gain[...]).astype(BF16)
    acc[:, : 2 * hidden] = jnp.zeros((slots, 2 * hidden), F32)
    acc[:, 2 * hidden :] = lanes
    bounds = [jnp.max(s).astype(jnp.int32) for s in starts]
    tile = min(slots, LANES)
    for e in range(expert_dev):
        for copy in copies[e]:
            copy.wait()
        for t in range(0, slots, tile):
            size = min(tile, slots - t)
            here = lax.broadcasted_iota(jnp.int32, (size, 1), 0) + t

            @pl.when((bounds[e] < t + size) & (bounds[e + 1] > t))
            def _():
                inside = (here >= bounds[e]) & (here < bounds[e + 1])
                rows = jnp.where(inside, scaled[t : t + size].astype(F32), 0.0).astype(BF16)
                acc[t : t + size, :hidden] += dot(rows, gate[e])
                acc[t : t + size, hidden : 2 * hidden] += dot(rows, up[e])
    for j in range(chips):
        to = 2 * partner(chip, j, chips)
        keep[j] = acc[pl.ds(pl.multiple_of((to + side) * share, 8), share), :]
        at = pl.multiple_of((to + 1 - side) * share, 8)
        give[j] = acc[pl.ds(at, share), :].astype(BF16)


def inner_kernel(model_width, *refs):
    sums, out = refs[:-1], refs[-1]
    hidden = out.shape[1]
    total = total_of([part[...] for part in sums])
    square = jnp.sum(total[:, 2 * hidden :], axis=1, keepdims=True)
    factor = lax.rsqrt(square / model_width + EPS)
    gate, up = total[:, :hidden] * factor, total[:, hidden : 2 * hidden] * factor
    out[...] = (jax.nn.silu(gate) * up).astype(BF16)


def down_kernel(chips, ep_count, expert_count, spot_ref, *refs):
    mine, other, refs = refs[:chips], refs[chips : 2 * chips], refs[2 * chips :]
    parts, down_hbm, outs = refs[:ep_count], refs[ep_count], refs[ep_count + 1 : 2 * ep_count + 1]
    down, code, wide, acc, sems = refs[2 * ep_count + 1 :]
    expert_dev, _, slice_width = down.shape
    copies = load_all(
        [down_hbm.at[e] for e in range(expert_dev)], [down.at[e] for e in range(expert_dev)], sems
    )
    side, chip = spot_ref[0], spot_ref[2]
    slots = acc.shape[0]
    share = mine[0].shape[0]
    rows = parts[0].shape[0]
    for j in range(ep_count):
        code[j * rows : (j + 1) * rows] = parts[j][:, slice_width:]
    token_count = code.shape[0]
    weights, taken, before, starts = placement(spot_ref, code[...], expert_dev, expert_count)
    for j in range(chips):
        source = 2 * back(chip, j, chips)
        for part, index in ((mine[j], source + side), (other[j], source + 1 - side)):
            wide[pl.ds(pl.multiple_of(index * share, 8), share), :] = part[...].astype(F32)
    bounds = [jnp.max(s).astype(jnp.int32) for s in starts]
    acc[...] = jnp.zeros(acc.shape, F32)
    tile = min(slots, LANES)
    for e in range(expert_dev):
        copies[e].wait()
        for t in range(0, slots, tile):
            size = min(tile, slots - t)
            here = lax.broadcasted_iota(jnp.int32, (size, 1), 0) + t

            @pl.when((bounds[e] < t + size) & (bounds[e + 1] > t))
            def _():
                inside = (here >= bounds[e]) & (here < bounds[e + 1])
                rows = jnp.where(inside, wide[t : t + size], 0.0).astype(BF16)
                acc[t : t + size, :] += dot(rows, down[e])
    slot = lax.broadcasted_iota(jnp.int32, (slots, token_count), 0).astype(F32)
    mix = jnp.zeros((slots, token_count), F32)
    for e in range(expert_dev):
        place = jnp.where(taken[e : e + 1] > 0, before[e : e + 1] + starts[e], -1.0)
        mix = mix + jnp.where(slot == place, weights[e : e + 1], 0.0)
    total = lax.dot_general(
        mix.astype(BF16),
        acc[...].astype(BF16),
        (((0,), (0,)), ((), ())),
        preferred_element_type=F32,
    )
    for j in range(ep_count):
        outs[j][...] = total[j * rows : (j + 1) * rows].astype(BF16)


def routed_experts(slots, spot, message, gain_own, model_width, expert_gate, expert_up, expert_down):
    chips, _ = tp_layout()
    ep_count = lax.axis_size("ep")
    expert_dev, slice_width, hidden = expert_gate.shape
    expert_count = expert_dev * ep_count
    seq_count, message_width = message[0].shape
    token_count = seq_count * ep_count
    share = slots // (2 * chips)
    columns = 2 * hidden + LANES
    keep, give = call(
        functools.partial(expert_kernel, chips, ep_count, expert_count),
        (
            jax.ShapeDtypeStruct((chips, share, columns), F32),
            jax.ShapeDtypeStruct((chips, share, columns), BF16),
        ),
        [IN_SMEM] + [IN_VMEM] * (1 + ep_count) + [IN_HBM] * 2,
        (
            pltpu.VMEM(expert_gate.shape, BF16),
            pltpu.VMEM(expert_up.shape, BF16),
            pltpu.VMEM((token_count, message_width), BF16),
            pltpu.VMEM((slots, slice_width), BF16),
            pltpu.VMEM((slots, columns), F32),
            pltpu.SemaphoreType.DMA((expert_dev, 2)),
        ),
    )(spot, gain_own, *message, *in_hbm(expert_gate, expert_up))
    sums = send_line(pair_sum(keep, give))
    inner = call(
        functools.partial(inner_kernel, model_width),
        jax.ShapeDtypeStruct((share, hidden), BF16),
        [IN_VMEM] * chips,
    )(*sums)
    mine, other = line_gather(inner)
    return call(
        functools.partial(down_kernel, chips, ep_count, expert_count),
        [jax.ShapeDtypeStruct((seq_count, slice_width), BF16)] * ep_count,
        [IN_SMEM] + [IN_VMEM] * (2 * chips + ep_count) + [IN_HBM],
        (
            pltpu.VMEM(expert_down.shape, BF16),
            pltpu.VMEM((token_count, message_width - slice_width), BF16),
            pltpu.VMEM((slots, hidden), F32),
            pltpu.VMEM((slots, slice_width), F32),
            pltpu.SemaphoreType.DMA((expert_dev,)),
        ),
    )(spot, *mine, *other, *message, *in_hbm(expert_down))


def local(
    tokens,
    norm_gain,
    ffn_gain,
    w_in,
    decay_rate,
    frequency,
    log_step,
    input_real,
    input_imag,
    readout_real,
    readout_imag,
    skip_gain,
    state_real,
    state_imag,
    w_out,
    shared_gate,
    shared_up,
    shared_down,
    expert_gate,
    expert_up,
    expert_down,
    routing,
    route_weight,
):
    seq_count, model_width = tokens.shape
    chips, _ = tp_layout()
    ep_count = lax.axis_size("ep")
    slice_width = model_width // (2 * chips)
    expert_dev = expert_gate.shape[0]
    expert_count = expert_dev * ep_count
    me = lax.axis_index("tp")
    offset = me * slice_width
    first = lax.axis_index("ep") * expert_dev
    at = jnp.arange(3)
    spot = jnp.where(at == 0, me % 2, jnp.where(at == 1, first, me // 2)).astype(jnp.int32)
    columns = (
        jax.ShapeDtypeStruct((chips, seq_count, slice_width), F32),
        jax.ShapeDtypeStruct((chips, seq_count, slice_width), BF16),
    )
    operands = (
        tokens,
        norm_gain[None],
        w_in,
        decay_rate[None],
        frequency[None],
        input_real,
        input_imag,
        state_real,
        state_imag,
        readout_real,
        readout_imag,
        skip_gain[None],
        w_out,
    )
    keep, give, new_real, new_imag = call(
        functools.partial(state_kernel, chips),
        columns
        + (
            jax.ShapeDtypeStruct(state_real.shape, F32),
            jax.ShapeDtypeStruct(state_imag.shape, F32),
        ),
        [IN_SMEM, IN_SMEM] + [IN_HBM] * len(operands),
        [pltpu.VMEM(x.shape, x.dtype) for x in operands]
        + [
            pltpu.VMEM((seq_count, w_out.shape[0]), BF16),
            pltpu.SemaphoreType.DMA((len(operands),)),
        ],
    )(spot, log_step, *in_hbm(*operands))
    arrived = send_line(pair_sum(keep, give))
    own_tokens = lax.dynamic_slice_in_dim(tokens, offset, slice_width, 1).astype(F32)
    resid_own = (own_tokens + total_of(arrived)).astype(BF16)
    gain_own = lax.dynamic_slice_in_dim(ffn_gain, offset, slice_width, 0)[None]

    top_count = routing.shape[1]
    weights = route_weight / jnp.sum(route_weight, axis=1, keepdims=True) * ROUTED_SCALE
    named = routing[:, :, None] == jnp.arange(expert_count, dtype=jnp.int32)
    dense = jnp.sum(jnp.where(named, weights[:, :, None], 0.0), axis=1)
    high = lax.reduce_precision(dense, 8, 7)
    code = jnp.concatenate([high, dense - high], axis=1)
    code = jnp.pad(code, ((0, 0), (0, -code.shape[1] % LANES))).astype(BF16)
    message = jnp.concatenate([resid_own, code], axis=1)
    message = send_ep([message] * ep_count)
    capacity = 2 * seq_count * top_count // expert_count
    slots = expert_dev * ep_count * capacity

    resid_mine, resid_other = line_gather(resid_own)
    combined = routed_experts(
        slots, spot, message, gain_own, model_width, expert_gate, expert_up, expert_down
    )
    keep, give = call(
        functools.partial(shared_kernel, chips),
        columns,
        [IN_SMEM] + [IN_VMEM] * (1 + 2 * chips) + [IN_HBM] * 3,
        [pltpu.VMEM(x.shape, BF16) for x in (shared_gate, shared_up, shared_down)]
        + [pltpu.SemaphoreType.DMA((3,))],
    )(
        spot,
        ffn_gain[None],
        *resid_mine,
        *resid_other,
        *in_hbm(shared_gate, shared_up, shared_down),
    )
    shared = send_line(pair_sum(keep, give))
    returned = send_ep(combined)
    mixed = (resid_own.astype(F32) + total_of(shared) + total_of(returned)).astype(BF16)
    return (mixed, new_real, new_imag)


def solution(mesh):
    placed = (
        P("ep", None),
        P(),
        P(),
        P(None, "tp"),
        P("tp"),
        P("tp"),
        P("tp"),
        P(None, "tp"),
        P(None, "tp"),
        P(None, "tp"),
        P(None, "tp"),
        P("tp"),
        P("ep", "tp"),
        P("ep", "tp"),
        P("tp", None),
        P(None, "tp"),
        P(None, "tp"),
        P("tp", None),
        P("ep", "tp", None),
        P("ep", "tp", None),
        P("ep", None, "tp"),
        P("ep", None),
        P("ep", None),
    )
    return jax.shard_map(
        local,
        mesh=mesh,
        in_specs=placed,
        out_specs=(P("ep", "tp"), P("ep", "tp"), P("ep", "tp")),
        check_vma=False,
    )
```

time: 198 us -> 99.4 us (0.50)
  waiting for transfers between devices: 96 us -> 39.8 us
  blocking collectives: 42.1 us -> 0 us
  starting transfers between devices: 4.25 us -> 36.3 us
  matrix products: 24.4 us -> 0 us
  Pallas kernels: 0 us -> 19.3 us
  between operations: 14 us -> 0.8 us
  local copies, waits for them, and re-layouts: 12 us -> 0.9 us
  other arithmetic: 4.21 us -> 2.11 us
    reduce_scatter x2 -> x0, waiting for transfers between devices: 53.2 us -> none  [the longest x1 33.1 us: local(): lax.psum_scatter(mixer_terms, 'tp', scatter_dimension=1, tiled=True)]
    psum x1 -> x0, waiting for transfers between devices: 42.7 us -> none  [local(): lax.psum(up_part.astype(jnp.bfloat16), 'tp').astype(jnp.float32)]
    ppermute x0 -> x32, waiting for transfers between devices: none -> 39.8 us  [the longest x15 29.1 us: send_line(): got.append(lax.ppermute(blocks[step], 'tp', pairs))]
    ppermute x0 -> x32, starting transfers between devices: none -> 36.3 us  [the longest x15 27.5 us: send_line(): got.append(lax.ppermute(blocks[step], 'tp', pairs))]
    dot_general x13 -> x0, matrix products: 24.4 us -> none  [the longest x1 4.04 us: local(): jnp.einsum('secd,edf->secf', arrived, expert_up, preferred_element_type=j...]
    pallas_call x0 -> x5, Pallas kernels: none -> 19.3 us  [the longest x1 6.07 us: routed_experts(): call(functools.partial(expert_kernel, chips, ep_count, expert_count), (ja...]
    all_gather x1 -> x0, blocking collectives: 16.5 us -> none  [local(): ffn_rows = lax.all_gather(rows_own, 'tp', axis=1, tiled=True)]
    psum x1 -> x0, blocking collectives: 13.9 us -> none  [local(): lax.psum(jnp.sum(resid_f * resid_f, axis=1, keepdims=True), 'tp')]
  transfers between devices with their start and end apart: 4 -> 32, of which waited for: 3 -> 18; matrix products, arithmetic and copies ran while one was open for 8% -> 1% of each run, Pallas kernels for 0% -> 7%
where the time goes in v1:
time: 99.4 us; the launch traced here: 99.3 us
  waiting for transfers between devices  39.8 us (40%)
  starting transfers between devices  36.3 us (37%)
  Pallas kernels  19.3 us (19%)
  other arithmetic  2.11 us (2%)
    ppermute x15, waiting for transfers between devices, send_line(): got.append(lax.ppermute(blocks[step], 'tp', pairs))  29.1 us
    ppermute x15, starting transfers between devices, send_line(): got.append(lax.ppermute(blocks[step], 'tp', pairs))  27.5 us
    ppermute x6, waiting for transfers between devices, send_ep(): got.append(lax.ppermute(blocks[step], 'ep', pairs))  7.56 us
    ppermute x6, starting transfers between devices, send_ep(): got.append(lax.ppermute(blocks[step], 'ep', pairs))  7.11 us
    pallas_call x1, Pallas kernels, routed_experts(): call(functools.partial(expert_kernel, chips, ep_count, expert_count), (ja...  6.07 us
    pallas_call x1, Pallas kernels, local(): call(functools.partial(state_kernel, chips), columns + (jax.ShapeDtypeStr...  5.98 us
    pallas_call x1, Pallas kernels, routed_experts(): call(functools.partial(down_kernel, chips, ep_count, expert_count), [jax....  4.11 us
    pallas_call x1, Pallas kernels, local(): call(functools.partial(shared_kernel, chips), columns, [IN_SMEM] + [IN_VM...  2.89 us
  transfers between devices with their start and end apart: 32, of which 18 were waited for; matrix products, arithmetic and copies ran while one was open for 1% of the time, Pallas kernels for 7%

profile of v1, /device:TPU:0, one launch (start us, length us, event | category | flops | bytes accessed | tf_op | source)
XLA Modules:
  0.0 99.3 jit_solution(9553416875808735502)
XLA Ops:
  1.3 6.0 %shard_map.238 = (f32[4,64,512]{2,1,0:T(8,128)S(1)}, bf16[4,64,512]{2,1,0:T(8,128)(2,1)S(1)}, f32[64,1024]{1,0:T(8,128)}, f32[64,1024]{1,0:T(8,128)}) custom-call(s32[3]{0:T(128)S(1)} %compare_select_fusion.1.spot_ref, f32[16]{0:T(128)S(1)} %copy-done.1, bf16[64,4096]{1,0:T(8,128)(2,1)} %refs_0_.1, f32[1,4096]{1,0:T(1,128)} %bitcast.38, ...), custom_call_target="tpu_custom_call" | custom-call | tf_op jit(solution)/shard_map/pallas_call | solution.py:452
  9.1 5.0 %collective-permute-start.3 = (bf16[64,512]{1,0:T(8,128)(2,1)S(1)}, bf16[64,512]{1,0:T(8,128)(2,1)S(1)}, u32[]{:S(2)}, u32[]{:S(2)}) collective-permute-start(bf16[64,512]{1,0:T(8,128)(2,1)S(1)} %get-tuple-element.35), channel_id=1, source_target_pairs={{0,6},{1,7},{2,4},{3,5},{4,2},{5,3},{6,0},{7,1},{8,14},{9,15},{10,... | collective-permute-start | bytes 196616 | tf_op jit(solution)/shard_map/ppermute | solution.py:51
  14.8 1.9 %collective-permute-done.3 = bf16[64,512]{1,0:T(8,128)(2,1)S(1)} collective-permute-done((bf16[64,512]{1,0:T(8,128)(2,1)S(1)}, bf16[64,512]{1,0:T(8,128)(2,1)S(1)}, u32[]{:S(2)}, u32[]{:S(2)}) %collective-permute-start.3) | collective-permute-done | bytes 65568 | tf_op jit(solution)/shard_map/ppermute | solution.py:51
  16.7 3.3 %collective-permute-done.2 = bf16[64,512]{1,0:T(8,128)(2,1)S(1)} collective-permute-done((bf16[64,512]{1,0:T(8,128)(2,1)S(1)}, bf16[64,512]{1,0:T(8,128)(2,1)S(1)}, u32[]{:S(2)}, u32[]{:S(2)}) %collective-permute-start.2) | collective-permute-done | bytes 65568 | tf_op jit(solution)/shard_map/ppermute | solution.py:51
  20.9 1.6 %collective-permute-start.15 = (bf16[64,640]{1,0:T(8,128)(2,1)S(1)}, bf16[64,640]{1,0:T(8,128)(2,1)S(1)}, u32[]{:S(2)}, u32[]{:S(2)}) collective-permute-start(bf16[64,640]{1,0:T(8,128)(2,1)S(1)} %pad_maximum_fusion.refs_0_.refs_8_), channel_id=1, source_target_pairs={{0,8},{8,0},{16,24},{24,16},{1,9},{9,1},{17,25},{25,17},{2,10},{10... | collective-permute-start | bytes 245768 | tf_op jit(solution)/shard_map/ppermute | solution.py:60
  22.5 1.5 %collective-permute-start.16 = (bf16[64,640]{1,0:T(8,128)(2,1)S(1)}, bf16[64,640]{1,0:T(8,128)(2,1)S(1)}, u32[]{:S(2)}, u32[]{:S(2)}) collective-permute-start(bf16[64,640]{1,0:T(8,128)(2,1)S(1)} %pad_maximum_fusion.refs_0_.refs_8_), channel_id=1, source_target_pairs={{0,16},{8,24},{16,0},{24,8},{1,17},{9,25},{17,1},{25,9},{2,18},{10... | collective-permute-start | bytes 245768 | tf_op jit(solution)/shard_map/ppermute | solution.py:60
  25.4 2.4 %collective-permute-done.16.refs_2_.refs_10_ = bf16[64,640]{1,0:T(8,128)(2,1)S(1)} collective-permute-done((bf16[64,640]{1,0:T(8,128)(2,1)S(1)}, bf16[64,640]{1,0:T(8,128)(2,1)S(1)}, u32[]{:S(2)}, u32[]{:S(2)}) %collective-permute-start.16) | collective-permute-done | bytes 81952 | tf_op jit(solution)/shard_map/ppermute | solution.py:60
  27.8 1.5 %collective-permute-done.17.refs_3_.refs_11_ = bf16[64,640]{1,0:T(8,128)(2,1)S(1)} collective-permute-done((bf16[64,640]{1,0:T(8,128)(2,1)S(1)}, bf16[64,640]{1,0:T(8,128)(2,1)S(1)}, u32[]{:S(2)}, u32[]{:S(2)}) %collective-permute-start.17) | collective-permute-done | bytes 81952 | tf_op jit(solution)/shard_map/ppermute | solution.py:60
  29.3 6.1 %shard_map.240 = (f32[4,64,2176]{2,1,0:T(8,128)S(1)}, bf16[4,64,2176]{2,1,0:T(8,128)(2,1)S(1)}) custom-call(s32[3]{0:T(128)S(1)} %compare_select_fusion.1.spot_ref, f32[1,512]{1,0:T(1,128)S(1)} %bitcast.37, bf16[64,640]{1,0:T(8,128)(2,1)S(1)} %pad_maximum_fusion.refs_0_.refs_8_, bf16[64,640]{1,0:T(8,128)(2,1)S(1)} %collective-permute-done.15.refs_1_.refs_9_, ...), custom_call_target="tpu_custom_call" | custom-call | tf_op jit(solution)/shard_map/pallas_call | solution.py:360
  36.7 1.9 %collective-permute-start.5 = (bf16[64,512]{1,0:T(8,128)(2,1)S(1)}, bf16[64,512]{1,0:T(8,128)(2,1)S(1)}, u32[]{:S(2)}, u32[]{:S(2)}) collective-permute-start(bf16[64,512]{1,0:T(8,128)(2,1)S(1)} %fusion.12.refs_0_), channel_id=1, source_target_pairs={{0,4},{1,5},{2,6},{3,7},{4,0},{5,1},{6,2},{7,3},{8,12},{9,13},{10,... | collective-permute-start | bytes 196616 | tf_op jit(solution)/shard_map/ppermute | solution.py:51
  38.6 1.3 %collective-permute-start.6 = (bf16[64,512]{1,0:T(8,128)(2,1)S(1)}, bf16[64,512]{1,0:T(8,128)(2,1)S(1)}, u32[]{:S(2)}, u32[]{:S(2)}) collective-permute-start(bf16[64,512]{1,0:T(8,128)(2,1)S(1)} %fusion.12.refs_0_), channel_id=1, source_target_pairs={{0,6},{1,7},{2,4},{3,5},{4,2},{5,3},{6,0},{7,1},{8,14},{9,15},{10,... | collective-permute-start | bytes 196616 | tf_op jit(solution)/shard_map/ppermute | solution.py:51
  40.5 2.8 %collective-permute-start.20 = (bf16[64,2176]{1,0:T(8,128)(2,1)S(1)}, bf16[64,2176]{1,0:T(8,128)(2,1)S(1)}, u32[]{:S(2)}, u32[]{:S(2)}) collective-permute-start(bf16[64,2176]{1,0:T(8,128)(2,1)S(1)} %get-tuple-element.28), channel_id=1, source_target_pairs={{0,4},{1,5},{2,6},{3,7},{4,0},{5,1},{6,2},{7,3},{8,12},{9,13},{10,... | collective-permute-start | bytes 835592 | tf_op jit(solution)/shard_map/ppermute | solution.py:51
  43.3 1.3 %collective-permute-start.21 = (bf16[64,2176]{1,0:T(8,128)(2,1)S(1)}, bf16[64,2176]{1,0:T(8,128)(2,1)S(1)}, u32[]{:S(2)}, u32[]{:S(2)}) collective-permute-start(bf16[64,2176]{1,0:T(8,128)(2,1)S(1)} %get-tuple-element.27), channel_id=1, source_target_pairs={{0,6},{1,7},{2,4},{3,5},{4,2},{5,3},{6,0},{7,1},{8,14},{9,15},{10,... | collective-permute-start | bytes 835592 | tf_op jit(solution)/shard_map/ppermute | solution.py:51
  47.9 2.9 %shard_map.239 = (f32[4,64,512]{2,1,0:T(8,128)S(1)}, bf16[4,64,512]{2,1,0:T(8,128)(2,1)S(1)}) custom-call(s32[3]{0:T(128)S(1)} %compare_select_fusion.1.spot_ref, f32[1,4096]{1,0:T(1,128)S(1)} %bitcast.36, bf16[64,512]{1,0:T(8,128)(2,1)S(1)} %fusion.12.refs_0_, bf16[64,512]{1,0:T(8,128)(2,1)S(1)} %collective-permute-done.4.refs_1_, ...), custom_call_target="tpu_custom_call" | custom-call | tf_op jit(solution)/shard_map/pallas_call | solution.py:487
  51.0 3.9 %collective-permute-done.19.refs_1_ = bf16[64,2176]{1,0:T(8,128)(2,1)S(1)} collective-permute-done((bf16[64,2176]{1,0:T(8,128)(2,1)S(1)}, bf16[64,2176]{1,0:T(8,128)(2,1)S(1)}, u32[]{:S(2)}, u32[]{:S(2)}) %collective-permute-start.19) | collective-permute-done | bytes 278560 | tf_op jit(solution)/shard_map/ppermute | solution.py:51
  54.9 9.4 %collective-permute-done.20.refs_2_ = bf16[64,2176]{1,0:T(8,128)(2,1)S(1)} collective-permute-done((bf16[64,2176]{1,0:T(8,128)(2,1)S(1)}, bf16[64,2176]{1,0:T(8,128)(2,1)S(1)}, u32[]{:S(2)}, u32[]{:S(2)}) %collective-permute-start.20) | collective-permute-done | bytes 278560 | tf_op jit(solution)/shard_map/ppermute | solution.py:51
  64.6 6.1 %collective-permute-start.22 = (bf16[64,1024]{1,0:T(8,128)(2,1)S(1)}, bf16[64,1024]{1,0:T(8,128)(2,1)S(1)}, u32[]{:S(2)}, u32[]{:S(2)}) collective-permute-start(bf16[64,1024]{1,0:T(8,128)(2,1)S(1)} %shard_map.241.refs_0_), channel_id=1, source_target_pairs={{0,2},{1,3},{2,0},{3,1},{4,6},{5,7},{6,4},{7,5},{8,10},{9,11},{10,... | collective-permute-start | bytes 393224 | tf_op jit(solution)/shard_map/ppermute | solution.py:51
  71.1 2.0 %collective-permute-start.24 = (bf16[64,1024]{1,0:T(8,128)(2,1)S(1)}, bf16[64,1024]{1,0:T(8,128)(2,1)S(1)}, u32[]{:S(2)}, u32[]{:S(2)}) collective-permute-start(bf16[64,1024]{1,0:T(8,128)(2,1)S(1)} %shard_map.241.refs_0_), channel_id=1, source_target_pairs={{0,6},{1,7},{2,4},{3,5},{4,2},{5,3},{6,0},{7,1},{8,14},{9,15},{10,... | collective-permute-start | bytes 393224 | tf_op jit(solution)/shard_map/ppermute | solution.py:51
  73.2 1.8 %collective-permute-done.22.refs_1_ = bf16[64,1024]{1,0:T(8,128)(2,1)S(1)} collective-permute-done((bf16[64,1024]{1,0:T(8,128)(2,1)S(1)}, bf16[64,1024]{1,0:T(8,128)(2,1)S(1)}, u32[]{:S(2)}, u32[]{:S(2)}) %collective-permute-start.22) | collective-permute-done | bytes 131104 | tf_op jit(solution)/shard_map/ppermute | solution.py:51
  74.9 8.1 %collective-permute-done.23.refs_2_ = bf16[64,1024]{1,0:T(8,128)(2,1)S(1)} collective-permute-done((bf16[64,1024]{1,0:T(8,128)(2,1)S(1)}, bf16[64,1024]{1,0:T(8,128)(2,1)S(1)}, u32[]{:S(2)}, u32[]{:S(2)}) %collective-permute-start.23) | collective-permute-done | bytes 131104 | tf_op jit(solution)/shard_map/ppermute | solution.py:51
  83.6 2.0 %collective-permute-start.14 = (bf16[64,512]{1,0:T(8,128)(2,1)S(1)}, bf16[64,512]{1,0:T(8,128)(2,1)S(1)}, u32[]{:S(2)}, u32[]{:S(2)}) collective-permute-start(bf16[64,512]{1,0:T(8,128)(2,1)S(1)} %get-tuple-element.32), channel_id=1, source_target_pairs={{0,6},{1,7},{2,4},{3,5},{4,2},{5,3},{6,0},{7,1},{8,14},{9,15},{10,... | collective-permute-start | bytes 196616 | tf_op jit(solution)/shard_map/ppermute | solution.py:51
  88.1 4.1 %shard_map.242 = (bf16[64,512]{1,0:T(8,128)(2,1)S(1)}, bf16[64,512]{1,0:T(8,128)(2,1)S(1)}, bf16[64,512]{1,0:T(8,128)(2,1)S(1)}, bf16[64,512]{1,0:T(8,128)(2,1)S(1)}) custom-call(s32[3]{0:T(128)S(1)} %compare_select_fusion.1.spot_ref, bf16[64,1024]{1,0:T(8,128)(2,1)S(1)} %shard_map.241.refs_0_, bf16[64,1024]{1,0:T(8,128)(2,1)S(1)} %collective-permute-done.22.refs_1_, ...), custom_call_target="tpu_custom_call" | custom-call | tf_op jit(solution)/shard_map/pallas_call | solution.py:383
  94.3 1.5 %collective-permute-start.29 = (bf16[64,512]{1,0:T(8,128)(2,1)S(1)}, bf16[64,512]{1,0:T(8,128)(2,1)S(1)}, u32[]{:S(2)}, u32[]{:S(2)}) collective-permute-start(bf16[64,512]{1,0:T(8,128)(2,1)S(1)} %get-tuple-element.22), channel_id=1, source_target_pairs={{0,8},{8,0},{16,24},{24,16},{1,9},{9,1},{17,25},{25,17},{2,10},{10... | collective-permute-start | bytes 196616 | tf_op jit(solution)/shard_map/ppermute | solution.py:60
  95.8 1.7 %collective-permute-done.31 = bf16[64,512]{1,0:T(8,128)(2,1)S(1)} collective-permute-done((bf16[64,512]{1,0:T(8,128)(2,1)S(1)}, bf16[64,512]{1,0:T(8,128)(2,1)S(1)}, u32[]{:S(2)}, u32[]{:S(2)}) %collective-permute-start.31) | collective-permute-done | bytes 65568 | tf_op jit(solution)/shard_map/ppermute | solution.py:60
  (69 shorter events, 18.2 us)
Async XLA Ops:
  9.1 7.6 %collective-permute-start.3 = (bf16[64,512]{1,0:T(8,128)(2,1)S(1)}, bf16[64,512]{1,0:T(8,128)(2,1)S(1)}, u32[]{:S(2)}, u32[]{:S(2)}) collective-permute-start(bf16[64,512]{1,0:T(8,128)(2,1)S(1)} %get-tuple-element.35), channel_id=1, source_target_pairs={{0,6},{1,7},{2,4},{3,5},{4,2},{5,3},{6,0},{7,1},{8,14},{9,15},{10,... | collective-permute-start | bytes 196616 | tf_op jit(solution)/shard_map/ppermute | solution.py:51
  14.1 5.9 %collective-permute-start.2 = (bf16[64,512]{1,0:T(8,128)(2,1)S(1)}, bf16[64,512]{1,0:T(8,128)(2,1)S(1)}, u32[]{:S(2)}, u32[]{:S(2)}) collective-permute-start(bf16[64,512]{1,0:T(8,128)(2,1)S(1)} %get-tuple-element.36), channel_id=1, source_target_pairs={{0,4},{1,5},{2,6},{3,7},{4,0},{5,1},{6,2},{7,3},{8,12},{9,13},{10,... | collective-permute-start | bytes 196616 | tf_op jit(solution)/shard_map/ppermute | solution.py:51
  14.1 5.9 %collective-permute-start.1 = (bf16[64,512]{1,0:T(8,128)(2,1)S(1)}, bf16[64,512]{1,0:T(8,128)(2,1)S(1)}, u32[]{:S(2)}, u32[]{:S(2)}) collective-permute-start(bf16[64,512]{1,0:T(8,128)(2,1)S(1)} %get-tuple-element.34), channel_id=1, source_target_pairs={{0,2},{1,3},{2,0},{3,1},{4,6},{5,7},{6,4},{7,5},{8,10},{9,11},{10,... | collective-permute-start | bytes 196616 | tf_op jit(solution)/shard_map/ppermute | solution.py:51
  22.5 5.3 %collective-permute-start.16 = (bf16[64,640]{1,0:T(8,128)(2,1)S(1)}, bf16[64,640]{1,0:T(8,128)(2,1)S(1)}, u32[]{:S(2)}, u32[]{:S(2)}) collective-permute-start(bf16[64,640]{1,0:T(8,128)(2,1)S(1)} %pad_maximum_fusion.refs_0_.refs_8_), channel_id=1, source_target_pairs={{0,16},{8,24},{16,0},{24,8},{1,17},{9,25},{17,1},{25,9},{2,18},{10... | collective-permute-start | bytes 245768 | tf_op jit(solution)/shard_map/ppermute | solution.py:60
  24.0 5.3 %collective-permute-start.17 = (bf16[64,640]{1,0:T(8,128)(2,1)S(1)}, bf16[64,640]{1,0:T(8,128)(2,1)S(1)}, u32[]{:S(2)}, u32[]{:S(2)}) collective-permute-start(bf16[64,640]{1,0:T(8,128)(2,1)S(1)} %pad_maximum_fusion.refs_0_.refs_8_), channel_id=1, source_target_pairs={{0,24},{8,16},{16,8},{24,0},{1,25},{9,17},{17,9},{25,1},{2,26},{10... | collective-permute-start | bytes 245768 | tf_op jit(solution)/shard_map/ppermute | solution.py:60
  35.5 7.8 %collective-permute-start.4 = (bf16[64,512]{1,0:T(8,128)(2,1)S(1)}, bf16[64,512]{1,0:T(8,128)(2,1)S(1)}, u32[]{:S(2)}, u32[]{:S(2)}) collective-permute-start(bf16[64,512]{1,0:T(8,128)(2,1)S(1)} %fusion.12.refs_0_), channel_id=1, source_target_pairs={{0,2},{1,3},{2,0},{3,1},{4,6},{5,7},{6,4},{7,5},{8,10},{9,11},{10,... | collective-permute-start | bytes 196616 | tf_op jit(solution)/shard_map/ppermute | solution.py:51
  36.7 8.0 %collective-permute-start.5 = (bf16[64,512]{1,0:T(8,128)(2,1)S(1)}, bf16[64,512]{1,0:T(8,128)(2,1)S(1)}, u32[]{:S(2)}, u32[]{:S(2)}) collective-permute-start(bf16[64,512]{1,0:T(8,128)(2,1)S(1)} %fusion.12.refs_0_), channel_id=1, source_target_pairs={{0,4},{1,5},{2,6},{3,7},{4,0},{5,1},{6,2},{7,3},{8,12},{9,13},{10,... | collective-permute-start | bytes 196616 | tf_op jit(solution)/shard_map/ppermute | solution.py:51
  38.6 6.8 %collective-permute-start.6 = (bf16[64,512]{1,0:T(8,128)(2,1)S(1)}, bf16[64,512]{1,0:T(8,128)(2,1)S(1)}, u32[]{:S(2)}, u32[]{:S(2)}) collective-permute-start(bf16[64,512]{1,0:T(8,128)(2,1)S(1)} %fusion.12.refs_0_), channel_id=1, source_target_pairs={{0,6},{1,7},{2,4},{3,5},{4,2},{5,3},{6,0},{7,1},{8,14},{9,15},{10,... | collective-permute-start | bytes 196616 | tf_op jit(solution)/shard_map/ppermute | solution.py:51
  40.2 14.7 %collective-permute-start.19 = (bf16[64,2176]{1,0:T(8,128)(2,1)S(1)}, bf16[64,2176]{1,0:T(8,128)(2,1)S(1)}, u32[]{:S(2)}, u32[]{:S(2)}) collective-permute-start(bf16[64,2176]{1,0:T(8,128)(2,1)S(1)} %get-tuple-element.29), channel_id=1, source_target_pairs={{0,2},{1,3},{2,0},{3,1},{4,6},{5,7},{6,4},{7,5},{8,10},{9,11},{10,... | collective-permute-start | bytes 835592 | tf_op jit(solution)/shard_map/ppermute | solution.py:51
  40.5 23.9 %collective-permute-start.20 = (bf16[64,2176]{1,0:T(8,128)(2,1)S(1)}, bf16[64,2176]{1,0:T(8,128)(2,1)S(1)}, u32[]{:S(2)}, u32[]{:S(2)}) collective-permute-start(bf16[64,2176]{1,0:T(8,128)(2,1)S(1)} %get-tuple-element.28), channel_id=1, source_target_pairs={{0,4},{1,5},{2,6},{3,7},{4,0},{5,1},{6,2},{7,3},{8,12},{9,13},{10,... | collective-permute-start | bytes 835592 | tf_op jit(solution)/shard_map/ppermute | solution.py:51
  43.3 21.0 %collective-permute-start.21 = (bf16[64,2176]{1,0:T(8,128)(2,1)S(1)}, bf16[64,2176]{1,0:T(8,128)(2,1)S(1)}, u32[]{:S(2)}, u32[]{:S(2)}) collective-permute-start(bf16[64,2176]{1,0:T(8,128)(2,1)S(1)} %get-tuple-element.27), channel_id=1, source_target_pairs={{0,6},{1,7},{2,4},{3,5},{4,2},{5,3},{6,0},{7,1},{8,14},{9,15},{10,... | collective-permute-start | bytes 835592 | tf_op jit(solution)/shard_map/ppermute | solution.py:51
  50.8 32.8 %collective-permute-start.11 = (bf16[4,64,512]{2,1,0:T(8,128)(2,1)S(1)}, bf16[4,64,512]{2,1,0:T(8,128)(2,1)S(1)}, u32[]{:S(2)}, u32[]{:S(2)}) collective-permute-start(bf16[4,64,512]{2,1,0:T(8,128)(2,1)S(1)} %get-tuple-element.18), channel_id=1, source_target_pairs={{0,1},{1,0},{2,3},{3,2},{4,5},{5,4},{6,7},{7,6},{8,9},{9,8},{10,11... | collective-permute-start | bytes 786440 | tf_op jit(solution)/shard_map/ppermute | solution.py:66
  64.6 10.3 %collective-permute-start.22 = (bf16[64,1024]{1,0:T(8,128)(2,1)S(1)}, bf16[64,1024]{1,0:T(8,128)(2,1)S(1)}, u32[]{:S(2)}, u32[]{:S(2)}) collective-permute-start(bf16[64,1024]{1,0:T(8,128)(2,1)S(1)} %shard_map.241.refs_0_), channel_id=1, source_target_pairs={{0,2},{1,3},{2,0},{3,1},{4,6},{5,7},{6,4},{7,5},{8,10},{9,11},{10,... | collective-permute-start | bytes 393224 | tf_op jit(solution)/shard_map/ppermute | solution.py:51
  70.7 12.3 %collective-permute-start.23 = (bf16[64,1024]{1,0:T(8,128)(2,1)S(1)}, bf16[64,1024]{1,0:T(8,128)(2,1)S(1)}, u32[]{:S(2)}, u32[]{:S(2)}) collective-permute-start(bf16[64,1024]{1,0:T(8,128)(2,1)S(1)} %shard_map.241.refs_0_), channel_id=1, source_target_pairs={{0,4},{1,5},{2,6},{3,7},{4,0},{5,1},{6,2},{7,3},{8,12},{9,13},{10,... | collective-permute-start | bytes 393224 | tf_op jit(solution)/shard_map/ppermute | solution.py:51
  71.1 11.9 %collective-permute-start.24 = (bf16[64,1024]{1,0:T(8,128)(2,1)S(1)}, bf16[64,1024]{1,0:T(8,128)(2,1)S(1)}, u32[]{:S(2)}, u32[]{:S(2)}) collective-permute-start(bf16[64,1024]{1,0:T(8,128)(2,1)S(1)} %shard_map.241.refs_0_), channel_id=1, source_target_pairs={{0,6},{1,7},{2,4},{3,5},{4,2},{5,3},{6,0},{7,1},{8,14},{9,15},{10,... | collective-permute-start | bytes 393224 | tf_op jit(solution)/shard_map/ppermute | solution.py:51
  73.2 12.5 %collective-permute-start.25 = (bf16[64,1024]{1,0:T(8,128)(2,1)S(1)}, bf16[64,1024]{1,0:T(8,128)(2,1)S(1)}, u32[]{:S(2)}, u32[]{:S(2)}) collective-permute-start(bf16[64,1024]{1,0:T(8,128)(2,1)S(1)} %shard_map.241.refs_0_), channel_id=1, source_target_pairs={{0,1},{1,0},{2,3},{3,2},{4,5},{5,4},{6,7},{7,6},{8,9},{9,8},{10,11... | collective-permute-start | bytes 393224 | tf_op jit(solution)/shard_map/ppermute | solution.py:73
  74.9 12.0 %collective-permute-start.26 = (bf16[64,1024]{1,0:T(8,128)(2,1)S(1)}, bf16[64,1024]{1,0:T(8,128)(2,1)S(1)}, u32[]{:S(2)}, u32[]{:S(2)}) collective-permute-start(bf16[64,1024]{1,0:T(8,128)(2,1)S(1)} %collective-permute-done.22.refs_1_), channel_id=1, source_target_pairs={{0,1},{1,0},{2,3},{3,2},{4,5},{5,4},{6,7},{7,6},{8,9},{9,8},{10,11... | collective-permute-start | bytes 393224 | tf_op jit(solution)/shard_map/ppermute | solution.py:73
  83.0 5.0 %collective-permute-start.27 = (bf16[64,1024]{1,0:T(8,128)(2,1)S(1)}, bf16[64,1024]{1,0:T(8,128)(2,1)S(1)}, u32[]{:S(2)}, u32[]{:S(2)}) collective-permute-start(bf16[64,1024]{1,0:T(8,128)(2,1)S(1)} %collective-permute-done.23.refs_2_), channel_id=1, source_target_pairs={{0,1},{1,0},{2,3},{3,2},{4,5},{5,4},{6,7},{7,6},{8,9},{9,8},{10,11... | collective-permute-start | bytes 393224 | tf_op jit(solution)/shard_map/ppermute | solution.py:73
  83.0 5.0 %collective-permute-start.28 = (bf16[64,1024]{1,0:T(8,128)(2,1)S(1)}, bf16[64,1024]{1,0:T(8,128)(2,1)S(1)}, u32[]{:S(2)}, u32[]{:S(2)}) collective-permute-start(bf16[64,1024]{1,0:T(8,128)(2,1)S(1)} %collective-permute-done.24.refs_3_), channel_id=1, source_target_pairs={{0,1},{1,0},{2,3},{3,2},{4,5},{5,4},{6,7},{7,6},{8,9},{9,8},{10,11... | collective-permute-start | bytes 393224 | tf_op jit(solution)/shard_map/ppermute | solution.py:73
  83.6 10.7 %collective-permute-start.14 = (bf16[64,512]{1,0:T(8,128)(2,1)S(1)}, bf16[64,512]{1,0:T(8,128)(2,1)S(1)}, u32[]{:S(2)}, u32[]{:S(2)}) collective-permute-start(bf16[64,512]{1,0:T(8,128)(2,1)S(1)} %get-tuple-element.32), channel_id=1, source_target_pairs={{0,6},{1,7},{2,4},{3,5},{4,2},{5,3},{6,0},{7,1},{8,14},{9,15},{10,... | collective-permute-start | bytes 196616 | tf_op jit(solution)/shard_map/ppermute | solution.py:51
  85.6 10.1 %collective-permute-start.13 = (bf16[64,512]{1,0:T(8,128)(2,1)S(1)}, bf16[64,512]{1,0:T(8,128)(2,1)S(1)}, u32[]{:S(2)}, u32[]{:S(2)}) collective-permute-start(bf16[64,512]{1,0:T(8,128)(2,1)S(1)} %get-tuple-element.33), channel_id=1, source_target_pairs={{0,4},{1,5},{2,6},{3,7},{4,0},{5,1},{6,2},{7,3},{8,12},{9,13},{10,... | collective-permute-start | bytes 196616 | tf_op jit(solution)/shard_map/ppermute | solution.py:51
  86.9 8.8 %collective-permute-start.12 = (bf16[64,512]{1,0:T(8,128)(2,1)S(1)}, bf16[64,512]{1,0:T(8,128)(2,1)S(1)}, u32[]{:S(2)}, u32[]{:S(2)}) collective-permute-start(bf16[64,512]{1,0:T(8,128)(2,1)S(1)} %get-tuple-element.31), channel_id=1, source_target_pairs={{0,2},{1,3},{2,0},{3,1},{4,6},{5,7},{6,4},{7,5},{8,10},{9,11},{10,... | collective-permute-start | bytes 196616 | tf_op jit(solution)/shard_map/ppermute | solution.py:51
  92.2 5.3 %collective-permute-start.31 = (bf16[64,512]{1,0:T(8,128)(2,1)S(1)}, bf16[64,512]{1,0:T(8,128)(2,1)S(1)}, u32[]{:S(2)}, u32[]{:S(2)}) collective-permute-start(bf16[64,512]{1,0:T(8,128)(2,1)S(1)} %get-tuple-element.24), channel_id=1, source_target_pairs={{0,24},{8,16},{16,8},{24,0},{1,25},{9,17},{17,9},{25,1},{2,26},{10... | collective-permute-start | bytes 196616 | tf_op jit(solution)/shard_map/ppermute | solution.py:60
  93.3 4.8 %collective-permute-start.30 = (bf16[64,512]{1,0:T(8,128)(2,1)S(1)}, bf16[64,512]{1,0:T(8,128)(2,1)S(1)}, u32[]{:S(2)}, u32[]{:S(2)}) collective-permute-start(bf16[64,512]{1,0:T(8,128)(2,1)S(1)} %get-tuple-element.23), channel_id=1, source_target_pairs={{0,16},{8,24},{16,0},{24,8},{1,17},{9,25},{17,1},{25,9},{2,18},{10... | collective-permute-start | bytes 196616 | tf_op jit(solution)/shard_map/ppermute | solution.py:60
  (12 other events, 57.0 us)

commit v2 on v1

--- a/solution.py
+++ b/solution.py
@@ -11,6 +11,7 @@
 EPS = 1e-06
 ROUTED_SCALE = 2.5
 LANES = 128
+ROWS = 16
 MIB = 1 << 20
 HIGH = lax.Precision.HIGHEST
 F32 = jnp.float32
@@ -105,11 +106,28 @@
     return copies
 
 
-def state_kernel(chips, spot_ref, log_step, *refs):
-    sources, (keep, give, new_re, new_im) = refs[:13], refs[13:17]
-    targets, acts, sems = refs[17:30], refs[30], refs[31]
+def preload_kernel(*refs):
+    count = len(refs) // 2
+    for copy in load_all(refs[:count], refs[count:-1], refs[-1]):
+        copy.wait()
+
+
+def preload(*arrays):
+    return pl.pallas_call(
+        preload_kernel,
+        out_shape=[pltpu.VMEM(x.shape, x.dtype) for x in arrays],
+        in_specs=[IN_HBM] * len(arrays),
+        out_specs=[IN_VMEM] * len(arrays),
+        scratch_shapes=[pltpu.SemaphoreType.DMA((len(arrays),))],
+        compiler_params=pltpu.CompilerParams(vmem_limit_bytes=MIB),
+    )(*in_hbm(*arrays))
+
+
+def state_kernel(chips, spot_ref, *refs):
+    sources, (keep, give, new_re, new_im) = refs[:14], refs[14:18]
+    targets, acts, sems = refs[18:32], refs[32], refs[33]
     (
-        tokens, gain, w_in, decay, omega, in_re, in_im, old_re, old_im, read_re, read_im, skip, w_out
+        tokens, gain, w_in, decay, omega, in_re, in_im, old_re, old_im, read_re, read_im, skip, w_out, log_step
     ) = targets
     copies = load_all(sources, targets, sems)
     copies[0].wait()
@@ -124,6 +142,7 @@
 
     group_of = lax.broadcasted_iota(jnp.int32, (1, states), 1) // width
     step = jnp.zeros((1, states), F32)
+    copies[13].wait()
     for g in range(groups):
         step = jnp.where(group_of == g, log_step[g], step)
     step = jnp.exp(step)
@@ -237,23 +256,33 @@
     return weights, taken, before, starts
 
 
+def expert_window(bounds, e, expert_dev, slots):
+    size = slots // expert_dev + ROWS
+    first = bounds[e] // ROWS * ROWS
+    row = lax.broadcasted_iota(jnp.int32, (size, 1), 0) + first
+    inside = (row >= bounds[e]) & (row < bounds[e + 1])
+    return pl.ds(pl.multiple_of(first, ROWS), size), inside
+
+
 def expert_kernel(chips, ep_count, expert_count, spot_ref, gain, *refs):
-    parts, (gate_hbm, up_hbm) = refs[:ep_count], refs[ep_count : ep_count + 2]
-    keep, give, gate, up, message, scaled, acc, sems = refs[ep_count + 2 :]
+    parts, (gate, up) = refs[:ep_count], refs[ep_count : ep_count + 2]
+    emitted, (over, message, scaled, acc) = refs[ep_count + 2 : -4], refs[-4:]
     expert_dev, slice_width, hidden = gate.shape
-    copies = [
-        load_all((gate_hbm.at[e], up_hbm.at[e]), (gate.at[e], up.at[e]), sems.at[e])
-        for e in range(expert_dev)
-    ]
     side, chip = spot_ref[0], spot_ref[2]
-    slots = acc.shape[0]
-    share = slots // (2 * chips)
+    slots = acc.shape[0] - ROWS
     rows = parts[0].shape[0]
     for j in range(ep_count):
         message[j * rows : (j + 1) * rows] = parts[j][...]
     token_count = message.shape[0]
     code = message[:, slice_width:]
     _, taken, before, starts = placement(spot_ref, code, expert_dev, expert_count)
+    named = jnp.sum((code > 0).astype(F32), axis=0, keepdims=True)
+    group = lax.broadcasted_iota(jnp.int32, named.shape, 1) // expert_dev
+    most = jnp.zeros((1, 1), F32)
+    for g in range(ep_count):
+        load = jnp.sum(jnp.where(group == g, named, 0.0), axis=1, keepdims=True)
+        most = jnp.maximum(most, load)
+    over[0] = (jnp.max(most) > 2 * chips * emitted[0].shape[1]).astype(jnp.int32)
     slot = lax.broadcasted_iota(jnp.int32, (slots, token_count), 0).astype(F32)
     hit = jnp.zeros((slots, token_count), F32)
     for e in range(expert_dev):
@@ -264,29 +293,33 @@
     lanes = squares[:, :LANES]
     for at in range(LANES, slice_width, LANES):
         lanes = lanes + squares[:, at : at + LANES]
-    scaled[...] = (picked * gain[...]).astype(BF16)
-    acc[:, : 2 * hidden] = jnp.zeros((slots, 2 * hidden), F32)
-    acc[:, 2 * hidden :] = lanes
+    scaled[:slots] = (picked * gain[...]).astype(BF16)
+    acc[:slots, 2 * hidden :] = lanes
     bounds = [jnp.max(s).astype(jnp.int32) for s in starts]
-    tile = min(slots, LANES)
+    for t in range(0, slots, LANES):
+        size = min(LANES, slots - t)
+
+        @pl.when(bounds[-1] < t + size)
+        def _():
+            acc[t : t + size, : 2 * hidden] = jnp.zeros((size, 2 * hidden), F32)
+
     for e in range(expert_dev):
-        for copy in copies[e]:
-            copy.wait()
-        for t in range(0, slots, tile):
-            size = min(tile, slots - t)
-            here = lax.broadcasted_iota(jnp.int32, (size, 1), 0) + t
-
-            @pl.when((bounds[e] < t + size) & (bounds[e + 1] > t))
-            def _():
-                inside = (here >= bounds[e]) & (here < bounds[e + 1])
-                rows = jnp.where(inside, scaled[t : t + size].astype(F32), 0.0).astype(BF16)
-                acc[t : t + size, :hidden] += dot(rows, gate[e])
-                acc[t : t + size, hidden : 2 * hidden] += dot(rows, up[e])
-    for j in range(chips):
-        to = 2 * partner(chip, j, chips)
-        keep[j] = acc[pl.ds(pl.multiple_of((to + side) * share, 8), share), :]
-        at = pl.multiple_of((to + 1 - side) * share, 8)
-        give[j] = acc[pl.ds(at, share), :].astype(BF16)
+        window, inside = expert_window(bounds, e, expert_dev, slots)
+        rows = scaled[window, :]
+        for at, weight in ((0, gate), (hidden, up)):
+            part = dot(rows, weight[e])
+            acc[window, at : at + hidden] = jnp.where(inside, part, acc[window, at : at + hidden])
+
+    base = 0
+    for keep, give in zip(emitted[::2], emitted[1::2]):
+        share = keep.shape[1]
+        for j in range(chips):
+            to = 2 * partner(chip, j, chips)
+            at = pl.multiple_of(base + (to + side) * share, 8)
+            keep[j] = acc[pl.ds(at, share), :]
+            at = pl.multiple_of(base + (to + 1 - side) * share, 8)
+            give[j] = acc[pl.ds(at, share), :].astype(BF16)
+        base += 2 * chips * share
 
 
 def inner_kernel(model_width, *refs):
@@ -301,14 +334,11 @@
 
 def down_kernel(chips, ep_count, expert_count, spot_ref, *refs):
     mine, other, refs = refs[:chips], refs[chips : 2 * chips], refs[2 * chips :]
-    parts, down_hbm, outs = refs[:ep_count], refs[ep_count], refs[ep_count + 1 : 2 * ep_count + 1]
-    down, code, wide, acc, sems = refs[2 * ep_count + 1 :]
+    parts, down, refs = refs[:ep_count], refs[ep_count], refs[ep_count + 1 :]
+    rest, outs, (code, wide, acc) = refs[: -ep_count - 3], refs[-ep_count - 3 : -3], refs[-3:]
     expert_dev, _, slice_width = down.shape
-    copies = load_all(
-        [down_hbm.at[e] for e in range(expert_dev)], [down.at[e] for e in range(expert_dev)], sems
-    )
     side, chip = spot_ref[0], spot_ref[2]
-    slots = acc.shape[0]
+    slots = acc.shape[0] - ROWS
     share = mine[0].shape[0]
     rows = parts[0].shape[0]
     for j in range(ep_count):
@@ -318,21 +348,18 @@
     for j in range(chips):
         source = 2 * back(chip, j, chips)
         for part, index in ((mine[j], source + side), (other[j], source + 1 - side)):
-            wide[pl.ds(pl.multiple_of(index * share, 8), share), :] = part[...].astype(F32)
+            wide[pl.ds(pl.multiple_of(index * share, 8), share), :] = part[...]
+            for more in rest:
+                extra = more.shape[1]
+                at = 2 * chips * share + index * extra
+                block = more[j if part is mine[j] else chips + j]
+                wide[pl.ds(pl.multiple_of(at, 8), extra), :] = block
     bounds = [jnp.max(s).astype(jnp.int32) for s in starts]
     acc[...] = jnp.zeros(acc.shape, F32)
-    tile = min(slots, LANES)
     for e in range(expert_dev):
-        copies[e].wait()
-        for t in range(0, slots, tile):
-            size = min(tile, slots - t)
-            here = lax.broadcasted_iota(jnp.int32, (size, 1), 0) + t
-
-            @pl.when((bounds[e] < t + size) & (bounds[e + 1] > t))
-            def _():
-                inside = (here >= bounds[e]) & (here < bounds[e + 1])
-                rows = jnp.where(inside, wide[t : t + size], 0.0).astype(BF16)
-                acc[t : t + size, :] += dot(rows, down[e])
+        window, inside = expert_window(bounds, e, expert_dev, slots)
+        part = dot(wide[window, :], down[e])
+        acc[window, :] = jnp.where(inside, part, acc[window, :])
     slot = lax.broadcasted_iota(jnp.int32, (slots, token_count), 0).astype(F32)
     mix = jnp.zeros((slots, token_count), F32)
     for e in range(expert_dev):
@@ -340,7 +367,7 @@
         mix = mix + jnp.where(slot == place, weights[e : e + 1], 0.0)
     total = lax.dot_general(
         mix.astype(BF16),
-        acc[...].astype(BF16),
+        acc[:slots].astype(BF16),
         (((0,), (0,)), ((), ())),
         preferred_element_type=F32,
     )
@@ -348,50 +375,69 @@
         outs[j][...] = total[j * rows : (j + 1) * rows].astype(BF16)
 
 
-def routed_experts(slots, spot, message, gain_own, model_width, expert_gate, expert_up, expert_down):
+def routed_experts(slots, spot, message, gain_own, model_width, gate_up, expert_down):
     chips, _ = tp_layout()
     ep_count = lax.axis_size("ep")
-    expert_dev, slice_width, hidden = expert_gate.shape
+    expert_dev, slice_width, hidden = gate_up[0].shape
     expert_count = expert_dev * ep_count
     seq_count, message_width = message[0].shape
     token_count = seq_count * ep_count
-    share = slots // (2 * chips)
     columns = 2 * hidden + LANES
-    keep, give = call(
+    tail = slots // 4
+    step = 16 * chips
+    shares = [slots // (2 * chips)]
+    if tail % step == 0 and (slots - tail) % step == 0:
+        shares = [(slots - tail) // (2 * chips), tail // (2 * chips)]
+    emitted = [
+        jax.ShapeDtypeStruct((chips, share, columns), kind) for share in shares for kind in (F32, BF16)
+    ]
+    *emitted, over = pl.pallas_call(
         functools.partial(expert_kernel, chips, ep_count, expert_count),
-        (
-            jax.ShapeDtypeStruct((chips, share, columns), F32),
-            jax.ShapeDtypeStruct((chips, share, columns), BF16),
-        ),
-        [IN_SMEM] + [IN_VMEM] * (1 + ep_count) + [IN_HBM] * 2,
-        (
-            pltpu.VMEM(expert_gate.shape, BF16),
-            pltpu.VMEM(expert_up.shape, BF16),
+        name="expert_in",
+        out_shape=emitted + [jax.ShapeDtypeStruct((1,), jnp.int32)],
+        in_specs=[IN_SMEM] + [IN_VMEM] * (3 + ep_count),
+        out_specs=[IN_VMEM] * len(emitted) + [IN_SMEM],
+        scratch_shapes=[
             pltpu.VMEM((token_count, message_width), BF16),
-            pltpu.VMEM((slots, slice_width), BF16),
-            pltpu.VMEM((slots, columns), F32),
-            pltpu.SemaphoreType.DMA((expert_dev, 2)),
-        ),
-    )(spot, gain_own, *message, *in_hbm(expert_gate, expert_up))
-    sums = send_line(pair_sum(keep, give))
-    inner = call(
-        functools.partial(inner_kernel, model_width),
-        jax.ShapeDtypeStruct((share, hidden), BF16),
-        [IN_VMEM] * chips,
-    )(*sums)
-    mine, other = line_gather(inner)
+            pltpu.VMEM((slots + ROWS, slice_width), BF16),
+            pltpu.VMEM((slots + ROWS, columns), F32),
+        ],
+        compiler_params=pltpu.CompilerParams(vmem_limit_bytes=20 * MIB),
+    )(spot, gain_own, *message, *gate_up)
+
+    def through(keep, give):
+        sums = send_line(pair_sum(keep, give))
+        inner = call(
+            functools.partial(inner_kernel, model_width),
+            jax.ShapeDtypeStruct((keep.shape[1], hidden), BF16),
+            [IN_VMEM] * chips,
+        )(*sums)
+        return line_gather(inner)
+
+    def more(keep, give):
+        mine, other = through(keep, give)
+        return jnp.stack(mine + other)
+
+    def none(keep, give):
+        return jnp.zeros((2 * chips, keep.shape[1], hidden), BF16)
+
+    mine, other = through(*emitted[:2])
+    rest = []
+    if len(shares) > 1:
+        rest = [lax.cond(over[0] > 0, more, none, *emitted[2:])]
+        rest[0], expert_down = lax.optimization_barrier((rest[0], expert_down))
+    (down,) = preload(expert_down)
     return call(
         functools.partial(down_kernel, chips, ep_count, expert_count),
         [jax.ShapeDtypeStruct((seq_count, slice_width), BF16)] * ep_count,
-        [IN_SMEM] + [IN_VMEM] * (2 * chips + ep_count) + [IN_HBM],
+        [IN_SMEM] + [IN_VMEM] * (2 * chips + ep_count + 1 + len(rest)),
         (
-            pltpu.VMEM(expert_down.shape, BF16),
             pltpu.VMEM((token_count, message_width - slice_width), BF16),
-            pltpu.VMEM((slots, hidden), F32),
-            pltpu.VMEM((slots, slice_width), F32),
-            pltpu.SemaphoreType.DMA((expert_dev,)),
+            pltpu.VMEM((slots + ROWS, hidden), BF16),
+            pltpu.VMEM((slots + ROWS, slice_width), F32),
         ),
-    )(spot, *mine, *other, *message, *in_hbm(expert_down))
+        limit=16,
+    )(spot, *mine, *other, *message, down, *rest)
 
 
 def local(
@@ -448,6 +494,7 @@
         readout_imag,
         skip_gain[None],
         w_out,
+        log_step,
     )
     keep, give, new_real, new_imag = call(
         functools.partial(state_kernel, chips),
@@ -456,14 +503,16 @@
             jax.ShapeDtypeStruct(state_real.shape, F32),
             jax.ShapeDtypeStruct(state_imag.shape, F32),
         ),
-        [IN_SMEM, IN_SMEM] + [IN_HBM] * len(operands),
-        [pltpu.VMEM(x.shape, x.dtype) for x in operands]
+        [IN_SMEM] + [IN_HBM] * len(operands),
+        [pltpu.VMEM(x.shape, x.dtype) for x in operands[:-1]]
         + [
+            pltpu.SMEM(log_step.shape, F32),
             pltpu.VMEM((seq_count, w_out.shape[0]), BF16),
             pltpu.SemaphoreType.DMA((len(operands),)),
         ],
-    )(spot, log_step, *in_hbm(*operands))
+    )(spot, *in_hbm(*operands))
     arrived = send_line(pair_sum(keep, give))
+    gate_up = preload(expert_gate, expert_up)
     own_tokens = lax.dynamic_slice_in_dim(tokens, offset, slice_width, 1).astype(F32)
     resid_own = (own_tokens + total_of(arrived)).astype(BF16)
     gain_own = lax.dynamic_slice_in_dim(ffn_gain, offset, slice_width, 0)[None]
@@ -482,7 +531,7 @@
 
     resid_mine, resid_other = line_gather(resid_own)
     combined = routed_experts(
-        slots, spot, message, gain_own, model_width, expert_gate, expert_up, expert_down
+        slots, spot, message, gain_own, model_width, gate_up, expert_down
     )
     keep, give = call(
         functools.partial(shared_kernel, chips),
@@ -497,7 +546,8 @@
         *resid_other,
         *in_hbm(shared_gate, shared_up, shared_down),
     )
-    shared = send_line(pair_sum(keep, give))
+    shared = pair_sum(keep, give)
+    shared = send_line(shared)
     returned = send_ep(combined)
     mixed = (resid_own.astype(F32) + total_of(shared) + total_of(returned)).astype(BF16)
     return (mixed, new_real, new_imag)

time: 99.4 us -> 95.3 us (0.959)
  waiting for transfers between devices: 39.8 us -> 33.6 us
  Pallas kernels: 19.3 us -> 20.6 us
  starting transfers between devices: 36.3 us -> 35.1 us
  other arithmetic: 2.11 us -> 3.24 us
    ppermute x6, waiting for transfers between devices: 7.56 us -> 4.05 us  [send_ep(): got.append(lax.ppermute(blocks[step], 'ep', pairs))]
    pallas_call x2 -> x4, Pallas kernels: 6.36 us -> 9.46 us  [the longest x2 5.68 us: preload(): pl.pallas_call(preload_kernel, out_shape=[pltpu.VMEM(x.shape, x.dtype) fo...]
    ppermute x8, waiting for transfers between devices: 2.2 us -> 0.02 us  [line_gather(): return (mine, [lax.ppermute(b, 'tp', swap) for b in mine])]
    pallas_call x1, Pallas kernels: 4.11 us -> 2.3 us  [routed_experts(): call(functools.partial(down_kernel, chips, ep_count, expert_count), [jax....]
    ppermute x15, starting transfers between devices: 27.5 us -> 25.8 us  [send_line(): got.append(lax.ppermute(blocks[step], 'tp', pairs))]
    convert_element_type x3, other arithmetic: 0.35 us -> 1.49 us  [pair_sum(): return [(keep[j] + got[j].astype(F32)).astype(BF16) for j in range(chips)]]
  transfers between devices with their start and end apart: 32 -> 32, of which waited for: 18 -> 13; matrix products, arithmetic and copies ran while one was open for 1% -> 3% of each run, Pallas kernels for 7% -> 12%
where the time goes in v2:
time: 95.3 us; the launch traced here: 95 us
  starting transfers between devices  35.1 us (37%)
  waiting for transfers between devices  33.6 us (35%)
  Pallas kernels  20.6 us (22%)
  other arithmetic  3.24 us (3%)
  between operations  1.5 us (2%)
  local copies, waits for them, and re-layouts  0.97 us (1%)
    ppermute x15, waiting for transfers between devices, send_line(): got.append(lax.ppermute(blocks[step], 'tp', pairs))  28.6 us
    ppermute x15, starting transfers between devices, send_line(): got.append(lax.ppermute(blocks[step], 'tp', pairs))  25.8 us
    ppermute x6, starting transfers between devices, send_ep(): got.append(lax.ppermute(blocks[step], 'ep', pairs))  7.11 us
    pallas_call x1, Pallas kernels, local(): call(functools.partial(state_kernel, chips), columns + (jax.ShapeDtypeStr...  6 us
    pallas_call x2, Pallas kernels, preload(): pl.pallas_call(preload_kernel, out_shape=[pltpu.VMEM(x.shape, x.dtype) fo...  5.68 us
    ppermute x6, waiting for transfers between devices, send_ep(): got.append(lax.ppermute(blocks[step], 'ep', pairs))  4.05 us
    pallas_call x1, Pallas kernels, routed_experts(): pl.pallas_call(functools.partial(expert_kernel, chips, ep_count, expert_c...  3.58 us
    pallas_call x1, Pallas kernels, local(): call(functools.partial(shared_kernel, chips), columns, [IN_SMEM] + [IN_VM...  2.87 us
  transfers between devices with their start and end apart: 32, of which 13 were waited for; matrix products, arithmetic and copies ran while one was open for 3% of the time, Pallas kernels for 12%

profile of v2, /device:TPU:0, one launch (start us, length us, event | category | flops | bytes accessed | tf_op | source)
XLA Modules:
  0.0 95.0 jit_solution(12246493745285992394)
XLA Ops:
  0.7 6.0 %shard_map.238 = (f32[4,64,512]{2,1,0:T(8,128)S(1)}, bf16[4,64,512]{2,1,0:T(8,128)(2,1)S(1)}, f32[64,1024]{1,0:T(8,128)}, f32[64,1024]{1,0:T(8,128)}) custom-call(s32[3]{0:T(128)S(1)} %compare_select_fusion.1.spot_ref, bf16[64,4096]{1,0:T(8,128)(2,1)} %refs_0_.2, f32[1,4096]{1,0:T(1,128)} %bitcast.63, bf16[4096,256]{1,0:T(8,128)(2,1)} %refs_2_.1, ...), custom_call_target="tpu_custom_call" | custom-call | tf_op jit(solution)/shard_map/pallas_call | solution.py:499
  8.5 5.0 %collective-permute-start.14 = (bf16[64,512]{1,0:T(8,128)(2,1)S(1)}, bf16[64,512]{1,0:T(8,128)(2,1)S(1)}, u32[]{:S(2)}, u32[]{:S(2)}) collective-permute-start(bf16[64,512]{1,0:T(8,128)(2,1)S(1)} %get-tuple-element.62), channel_id=1, source_target_pairs={{0,6},{1,7},{2,4},{3,5},{4,2},{5,3},{6,0},{7,1},{8,14},{9,15},{10,... | collective-permute-start | bytes 196616 | tf_op jit(solution)/shard_map/ppermute | solution.py:52
  14.2 1.9 %collective-permute-done.14 = bf16[64,512]{1,0:T(8,128)(2,1)S(1)} collective-permute-done((bf16[64,512]{1,0:T(8,128)(2,1)S(1)}, bf16[64,512]{1,0:T(8,128)(2,1)S(1)}, u32[]{:S(2)}, u32[]{:S(2)}) %collective-permute-start.14) | collective-permute-done | bytes 65568 | tf_op jit(solution)/shard_map/ppermute | solution.py:52
  16.1 3.3 %collective-permute-done.13 = bf16[64,512]{1,0:T(8,128)(2,1)S(1)} collective-permute-done((bf16[64,512]{1,0:T(8,128)(2,1)S(1)}, bf16[64,512]{1,0:T(8,128)(2,1)S(1)}, u32[]{:S(2)}, u32[]{:S(2)}) %collective-permute-start.13) | collective-permute-done | bytes 65568 | tf_op jit(solution)/shard_map/ppermute | solution.py:52
  20.3 1.6 %collective-permute-start.26 = (bf16[64,640]{1,0:T(8,128)(2,1)S(1)}, bf16[64,640]{1,0:T(8,128)(2,1)S(1)}, u32[]{:S(2)}, u32[]{:S(2)}) collective-permute-start(bf16[64,640]{1,0:T(8,128)(2,1)S(1)} %pad_maximum_fusion.refs_0_.refs_8_), channel_id=1, source_target_pairs={{0,8},{8,0},{16,24},{24,16},{1,9},{9,1},{17,25},{25,17},{2,10},{10... | collective-permute-start | bytes 245768 | tf_op jit(solution)/shard_map/ppermute | solution.py:61
  21.9 1.5 %collective-permute-start.27 = (bf16[64,640]{1,0:T(8,128)(2,1)S(1)}, bf16[64,640]{1,0:T(8,128)(2,1)S(1)}, u32[]{:S(2)}, u32[]{:S(2)}) collective-permute-start(bf16[64,640]{1,0:T(8,128)(2,1)S(1)} %pad_maximum_fusion.refs_0_.refs_8_), channel_id=1, source_target_pairs={{0,16},{8,24},{16,0},{24,8},{1,17},{9,25},{17,1},{25,9},{2,18},{10... | collective-permute-start | bytes 245768 | tf_op jit(solution)/shard_map/ppermute | solution.py:61
  23.9 3.5 %shard_map.240 = (bf16[4,512,1024]{2,1,0:T(8,128)(2,1)S(1)}, bf16[4,512,1024]{2,1,0:T(8,128)(2,1)S(1)}) custom-call(bf16[4,512,1024]{2,1,0:T(8,128)(2,1)} %refs_0_.3, bf16[4,512,1024]{2,1,0:T(8,128)(2,1)} %refs_1_.1), custom_call_target="tpu_custom_call" | custom-call | tf_op jit(solution)/shard_map/pallas_call | solution.py:116
  28.7 3.6 %expert_in.1 = (f32[4,48,2176]{2,1,0:T(8,128)S(1)}, bf16[4,48,2176]{2,1,0:T(8,128)(2,1)S(1)}, f32[4,16,2176]{2,1,0:T(8,128)S(1)}, bf16[4,16,2176]{2,1,0:T(8,128)(2,1)S(1)}, s32[1]{0:T(128)}) custom-call(s32[3]{0:T(128)S(1)} %compare_select_fusion.1.spot_ref, f32[1,512]{1,0:T(1,128)S(1)} %bitcast.62, bf16[64,640]{1,0:T(8,128)(2,1)S(1)} %pad_maximum_fusion.refs_0_.refs_8_, ...), custom_call_target="tpu_custom_call" | custom-call | tf_op jit(solution)/shard_map/expert_in/pallas_call | solution.py:394
  34.9 1.9 %collective-permute-start.16 = (bf16[64,512]{1,0:T(8,128)(2,1)S(1)}, bf16[64,512]{1,0:T(8,128)(2,1)S(1)}, u32[]{:S(2)}, u32[]{:S(2)}) collective-permute-start(bf16[64,512]{1,0:T(8,128)(2,1)S(1)} %fusion.16.refs_0_), channel_id=1, source_target_pairs={{0,4},{1,5},{2,6},{3,7},{4,0},{5,1},{6,2},{7,3},{8,12},{9,13},{10,... | collective-permute-start | bytes 196616 | tf_op jit(solution)/shard_map/ppermute | solution.py:52
  38.7 4.6 %collective-permute-done.16.refs_2_ = bf16[64,512]{1,0:T(8,128)(2,1)S(1)} collective-permute-done((bf16[64,512]{1,0:T(8,128)(2,1)S(1)}, bf16[64,512]{1,0:T(8,128)(2,1)S(1)}, u32[]{:S(2)}, u32[]{:S(2)}) %collective-permute-start.16) | collective-permute-done | bytes 65568 | tf_op jit(solution)/shard_map/ppermute | solution.py:52
  43.8 1.4 %fusion.7 = (bf16[48,2176]{1,0:T(8,128)(2,1)S(1)}, bf16[48,2176]{1,0:T(8,128)(2,1)S(1)}, bf16[48,2176]{1,0:T(8,128)(2,1)S(1)}, bf16[48,2176]{1,0:T(8,128)(2,1)S(1)}) fusion(f32[4,48,2176]{2,1,0:T(8,128)S(1)} %get-tuple-element.37, bf16[4,48,2176]{2,1,0:T(8,128)(2,1)} %collective-permute-done.29), kind=kLoop, calls=%fused_computation.23 | loop fusion | flops 1253376 | bytes 3342336 | tf_op jit(solution)/shard_map/convert_element_type | solution.py:68
  47.6 2.1 %collective-permute-start.32 = (bf16[48,2176]{1,0:T(8,128)(2,1)S(1)}, bf16[48,2176]{1,0:T(8,128)(2,1)S(1)}, u32[]{:S(2)}, u32[]{:S(2)}) collective-permute-start(bf16[48,2176]{1,0:T(8,128)(2,1)S(1)} %get-tuple-element.54), channel_id=1, source_target_pairs={{0,6},{1,7},{2,4},{3,5},{4,2},{5,3},{6,0},{7,1},{8,14},{9,15},{10,... | collective-permute-start | bytes 626696 | tf_op jit(solution)/shard_map/ppermute | solution.py:52
  49.7 2.9 %shard_map.239 = (f32[4,64,512]{2,1,0:T(8,128)S(1)}, bf16[4,64,512]{2,1,0:T(8,128)(2,1)S(1)}) custom-call(s32[3]{0:T(128)S(1)} %compare_select_fusion.1.spot_ref, f32[1,4096]{1,0:T(1,128)S(1)} %bitcast.61, bf16[64,512]{1,0:T(8,128)(2,1)S(1)} %fusion.16.refs_0_, bf16[64,512]{1,0:T(8,128)(2,1)S(1)} %collective-permute-done.15.refs_1_, ...), custom_call_target="tpu_custom_call" | custom-call | tf_op jit(solution)/shard_map/pallas_call | solution.py:536
  52.7 3.3 %collective-permute-done.30.refs_1_ = bf16[48,2176]{1,0:T(8,128)(2,1)S(1)} collective-permute-done((bf16[48,2176]{1,0:T(8,128)(2,1)S(1)}, bf16[48,2176]{1,0:T(8,128)(2,1)S(1)}, u32[]{:S(2)}, u32[]{:S(2)}) %collective-permute-start.30) | collective-permute-done | bytes 208928 | tf_op jit(solution)/shard_map/ppermute | solution.py:52
  56.0 8.2 %collective-permute-done.31.refs_2_ = bf16[48,2176]{1,0:T(8,128)(2,1)S(1)} collective-permute-done((bf16[48,2176]{1,0:T(8,128)(2,1)S(1)}, bf16[48,2176]{1,0:T(8,128)(2,1)S(1)}, u32[]{:S(2)}, u32[]{:S(2)}) %collective-permute-start.31) | collective-permute-done | bytes 208928 | tf_op jit(solution)/shard_map/ppermute | solution.py:52
  64.4 4.4 %collective-permute-start.33 = (bf16[48,1024]{1,0:T(8,128)(2,1)S(1)}, bf16[48,1024]{1,0:T(8,128)(2,1)S(1)}, u32[]{:S(2)}, u32[]{:S(2)}) collective-permute-start(bf16[48,1024]{1,0:T(8,128)(2,1)S(1)} %shard_map.241.refs_0_), channel_id=1, source_target_pairs={{0,2},{1,3},{2,0},{3,1},{4,6},{5,7},{6,4},{7,5},{8,10},{9,11},{10,... | collective-permute-start | bytes 294920 | tf_op jit(solution)/shard_map/ppermute | solution.py:52
  69.1 2.1 %collective-permute-start.35 = (bf16[48,1024]{1,0:T(8,128)(2,1)S(1)}, bf16[48,1024]{1,0:T(8,128)(2,1)S(1)}, u32[]{:S(2)}, u32[]{:S(2)}) collective-permute-start(bf16[48,1024]{1,0:T(8,128)(2,1)S(1)} %shard_map.241.refs_0_), channel_id=1, source_target_pairs={{0,6},{1,7},{2,4},{3,5},{4,2},{5,3},{6,0},{7,1},{8,14},{9,15},{10,... | collective-permute-start | bytes 294920 | tf_op jit(solution)/shard_map/ppermute | solution.py:52
  71.9 6.4 %collective-permute-done.34.refs_2_ = bf16[48,1024]{1,0:T(8,128)(2,1)S(1)} collective-permute-done((bf16[48,1024]{1,0:T(8,128)(2,1)S(1)}, bf16[48,1024]{1,0:T(8,128)(2,1)S(1)}, u32[]{:S(2)}, u32[]{:S(2)}) %collective-permute-start.34) | collective-permute-done | bytes 98336 | tf_op jit(solution)/shard_map/ppermute | solution.py:52
  78.9 2.0 %collective-permute-start.25 = (bf16[64,512]{1,0:T(8,128)(2,1)S(1)}, bf16[64,512]{1,0:T(8,128)(2,1)S(1)}, u32[]{:S(2)}, u32[]{:S(2)}) collective-permute-start(bf16[64,512]{1,0:T(8,128)(2,1)S(1)} %get-tuple-element.59), channel_id=1, source_target_pairs={{0,6},{1,7},{2,4},{3,5},{4,2},{5,3},{6,0},{7,1},{8,14},{9,15},{10,... | collective-permute-start | bytes 196616 | tf_op jit(solution)/shard_map/ppermute | solution.py:52
  80.9 2.2 %shard_map.242.refs_12_ = bf16[4,1024,512]{2,1,0:T(8,128)(2,1)S(1)} custom-call(bf16[4,1024,512]{2,1,0:T(8,128)(2,1)} %refs_0_.4), custom_call_target="tpu_custom_call" | custom-call | tf_op jit(solution)/shard_map/pallas_call | solution.py:116
  84.2 1.5 %collective-permute-start.23 = (bf16[64,512]{1,0:T(8,128)(2,1)S(1)}, bf16[64,512]{1,0:T(8,128)(2,1)S(1)}, u32[]{:S(2)}, u32[]{:S(2)}) collective-permute-start(bf16[64,512]{1,0:T(8,128)(2,1)S(1)} %get-tuple-element.58), channel_id=1, source_target_pairs={{0,2},{1,3},{2,0},{3,1},{4,6},{5,7},{6,4},{7,5},{8,10},{9,11},{10,... | collective-permute-start | bytes 196616 | tf_op jit(solution)/shard_map/ppermute | solution.py:52
  85.7 2.3 %shard_map.243 = (bf16[64,512]{1,0:T(8,128)(2,1)S(1)}, bf16[64,512]{1,0:T(8,128)(2,1)S(1)}, bf16[64,512]{1,0:T(8,128)(2,1)S(1)}, bf16[64,512]{1,0:T(8,128)(2,1)S(1)}) custom-call(s32[3]{0:T(128)S(1)} %compare_select_fusion.1.spot_ref, bf16[48,1024]{1,0:T(8,128)(2,1)S(1)} %shard_map.241.refs_0_, bf16[48,1024]{1,0:T(8,128)(2,1)S(1)} %collective-permute-done.33.refs_1_, ...), custom_call_target="tpu_custom_call" | custom-call | tf_op jit(solution)/shard_map/pallas_call | solution.py:430
  90.1 1.5 %collective-permute-start.40 = (bf16[64,512]{1,0:T(8,128)(2,1)S(1)}, bf16[64,512]{1,0:T(8,128)(2,1)S(1)}, u32[]{:S(2)}, u32[]{:S(2)}) collective-permute-start(bf16[64,512]{1,0:T(8,128)(2,1)S(1)} %get-tuple-element.45), channel_id=1, source_target_pairs={{0,8},{8,0},{16,24},{24,16},{1,9},{9,1},{17,25},{25,17},{2,10},{10... | collective-permute-start | bytes 196616 | tf_op jit(solution)/shard_map/ppermute | solution.py:61
  91.6 1.8 %collective-permute-done.42 = bf16[64,512]{1,0:T(8,128)(2,1)S(1)} collective-permute-done((bf16[64,512]{1,0:T(8,128)(2,1)S(1)}, bf16[64,512]{1,0:T(8,128)(2,1)S(1)}, u32[]{:S(2)}, u32[]{:S(2)}) %collective-permute-start.42) | collective-permute-done | bytes 65568 | tf_op jit(solution)/shard_map/ppermute | solution.py:61
  (71 shorter events, 19.3 us)
Async XLA Ops:
  8.5 7.6 %collective-permute-start.14 = (bf16[64,512]{1,0:T(8,128)(2,1)S(1)}, bf16[64,512]{1,0:T(8,128)(2,1)S(1)}, u32[]{:S(2)}, u32[]{:S(2)}) collective-permute-start(bf16[64,512]{1,0:T(8,128)(2,1)S(1)} %get-tuple-element.62), channel_id=1, source_target_pairs={{0,6},{1,7},{2,4},{3,5},{4,2},{5,3},{6,0},{7,1},{8,14},{9,15},{10,... | collective-permute-start | bytes 196616 | tf_op jit(solution)/shard_map/ppermute | solution.py:52
  13.5 5.9 %collective-permute-start.13 = (bf16[64,512]{1,0:T(8,128)(2,1)S(1)}, bf16[64,512]{1,0:T(8,128)(2,1)S(1)}, u32[]{:S(2)}, u32[]{:S(2)}) collective-permute-start(bf16[64,512]{1,0:T(8,128)(2,1)S(1)} %get-tuple-element.63), channel_id=1, source_target_pairs={{0,4},{1,5},{2,6},{3,7},{4,0},{5,1},{6,2},{7,3},{8,12},{9,13},{10,... | collective-permute-start | bytes 196616 | tf_op jit(solution)/shard_map/ppermute | solution.py:52
  20.3 7.1 %collective-permute-start.26 = (bf16[64,640]{1,0:T(8,128)(2,1)S(1)}, bf16[64,640]{1,0:T(8,128)(2,1)S(1)}, u32[]{:S(2)}, u32[]{:S(2)}) collective-permute-start(bf16[64,640]{1,0:T(8,128)(2,1)S(1)} %pad_maximum_fusion.refs_0_.refs_8_), channel_id=1, source_target_pairs={{0,8},{8,0},{16,24},{24,16},{1,9},{9,1},{17,25},{25,17},{2,10},{10... | collective-permute-start | bytes 245768 | tf_op jit(solution)/shard_map/ppermute | solution.py:61
  32.3 11.5 %collective-permute-start.29 = (bf16[4,48,2176]{2,1,0:T(8,128)(2,1)S(1)}, bf16[4,48,2176]{2,1,0:T(8,128)(2,1)}, u32[]{:S(2)}, u32[]{:S(2)}) collective-permute-start(bf16[4,48,2176]{2,1,0:T(8,128)(2,1)S(1)} %get-tuple-element.38), channel_id=1, source_target_pairs={{0,1},{1,0},{2,3},{3,2},{4,5},{5,4},{6,7},{7,6},{8,9},{9,8},{10,11... | collective-permute-start | bytes 2506760 | tf_op jit(solution)/shard_map/ppermute | solution.py:67
  34.9 8.5 %collective-permute-start.16 = (bf16[64,512]{1,0:T(8,128)(2,1)S(1)}, bf16[64,512]{1,0:T(8,128)(2,1)S(1)}, u32[]{:S(2)}, u32[]{:S(2)}) collective-permute-start(bf16[64,512]{1,0:T(8,128)(2,1)S(1)} %fusion.16.refs_0_), channel_id=1, source_target_pairs={{0,4},{1,5},{2,6},{3,7},{4,0},{5,1},{6,2},{7,3},{8,12},{9,13},{10,... | collective-permute-start | bytes 196616 | tf_op jit(solution)/shard_map/ppermute | solution.py:52
  36.8 6.5 %collective-permute-start.17 = (bf16[64,512]{1,0:T(8,128)(2,1)S(1)}, bf16[64,512]{1,0:T(8,128)(2,1)S(1)}, u32[]{:S(2)}, u32[]{:S(2)}) collective-permute-start(bf16[64,512]{1,0:T(8,128)(2,1)S(1)} %fusion.16.refs_0_), channel_id=1, source_target_pairs={{0,6},{1,7},{2,4},{3,5},{4,2},{5,3},{6,0},{7,1},{8,14},{9,15},{10,... | collective-permute-start | bytes 196616 | tf_op jit(solution)/shard_map/ppermute | solution.py:52
  38.2 8.1 %collective-permute-start.18 = (bf16[64,512]{1,0:T(8,128)(2,1)S(1)}, bf16[64,512]{1,0:T(8,128)(2,1)S(1)}, u32[]{:S(2)}, u32[]{:S(2)}) collective-permute-start(bf16[64,512]{1,0:T(8,128)(2,1)S(1)} %fusion.16.refs_0_), channel_id=1, source_target_pairs={{0,1},{1,0},{2,3},{3,2},{4,5},{5,4},{6,7},{7,6},{8,9},{9,8},{10,11... | collective-permute-start | bytes 196616 | tf_op jit(solution)/shard_map/ppermute | solution.py:74
  38.3 9.3 %collective-permute-start.19 = (bf16[64,512]{1,0:T(8,128)(2,1)S(1)}, bf16[64,512]{1,0:T(8,128)(2,1)S(1)}, u32[]{:S(2)}, u32[]{:S(2)}) collective-permute-start(bf16[64,512]{1,0:T(8,128)(2,1)S(1)} %collective-permute-done.15.refs_1_), channel_id=1, source_target_pairs={{0,1},{1,0},{2,3},{3,2},{4,5},{5,4},{6,7},{7,6},{8,9},{9,8},{10,11... | collective-permute-start | bytes 196616 | tf_op jit(solution)/shard_map/ppermute | solution.py:74
  43.3 6.4 %collective-permute-start.20 = (bf16[64,512]{1,0:T(8,128)(2,1)S(1)}, bf16[64,512]{1,0:T(8,128)(2,1)S(1)}, u32[]{:S(2)}, u32[]{:S(2)}) collective-permute-start(bf16[64,512]{1,0:T(8,128)(2,1)S(1)} %collective-permute-done.16.refs_2_), channel_id=1, source_target_pairs={{0,1},{1,0},{2,3},{3,2},{4,5},{5,4},{6,7},{7,6},{8,9},{9,8},{10,11... | collective-permute-start | bytes 196616 | tf_op jit(solution)/shard_map/ppermute | solution.py:74
  43.3 6.4 %collective-permute-start.21 = (bf16[64,512]{1,0:T(8,128)(2,1)S(1)}, bf16[64,512]{1,0:T(8,128)(2,1)S(1)}, u32[]{:S(2)}, u32[]{:S(2)}) collective-permute-start(bf16[64,512]{1,0:T(8,128)(2,1)S(1)} %collective-permute-done.17.refs_3_), channel_id=1, source_target_pairs={{0,1},{1,0},{2,3},{3,2},{4,5},{5,4},{6,7},{7,6},{8,9},{9,8},{10,11... | collective-permute-start | bytes 196616 | tf_op jit(solution)/shard_map/ppermute | solution.py:74
  45.2 10.8 %collective-permute-start.30 = (bf16[48,2176]{1,0:T(8,128)(2,1)S(1)}, bf16[48,2176]{1,0:T(8,128)(2,1)S(1)}, u32[]{:S(2)}, u32[]{:S(2)}) collective-permute-start(bf16[48,2176]{1,0:T(8,128)(2,1)S(1)} %get-tuple-element.56), channel_id=1, source_target_pairs={{0,2},{1,3},{2,0},{3,1},{4,6},{5,7},{6,4},{7,5},{8,10},{9,11},{10,... | collective-permute-start | bytes 626696 | tf_op jit(solution)/shard_map/ppermute | solution.py:52
  46.2 17.9 %collective-permute-start.31 = (bf16[48,2176]{1,0:T(8,128)(2,1)S(1)}, bf16[48,2176]{1,0:T(8,128)(2,1)S(1)}, u32[]{:S(2)}, u32[]{:S(2)}) collective-permute-start(bf16[48,2176]{1,0:T(8,128)(2,1)S(1)} %get-tuple-element.55), channel_id=1, source_target_pairs={{0,4},{1,5},{2,6},{3,7},{4,0},{5,1},{6,2},{7,3},{8,12},{9,13},{10,... | collective-permute-start | bytes 626696 | tf_op jit(solution)/shard_map/ppermute | solution.py:52
  47.6 16.6 %collective-permute-start.32 = (bf16[48,2176]{1,0:T(8,128)(2,1)S(1)}, bf16[48,2176]{1,0:T(8,128)(2,1)S(1)}, u32[]{:S(2)}, u32[]{:S(2)}) collective-permute-start(bf16[48,2176]{1,0:T(8,128)(2,1)S(1)} %get-tuple-element.54), channel_id=1, source_target_pairs={{0,6},{1,7},{2,4},{3,5},{4,2},{5,3},{6,0},{7,1},{8,14},{9,15},{10,... | collective-permute-start | bytes 626696 | tf_op jit(solution)/shard_map/ppermute | solution.py:52
  52.6 26.3 %collective-permute-start.22 = (bf16[4,64,512]{2,1,0:T(8,128)(2,1)S(1)}, bf16[4,64,512]{2,1,0:T(8,128)(2,1)S(1)}, u32[]{:S(2)}, u32[]{:S(2)}) collective-permute-start(bf16[4,64,512]{2,1,0:T(8,128)(2,1)S(1)} %get-tuple-element.34), channel_id=1, source_target_pairs={{0,1},{1,0},{2,3},{3,2},{4,5},{5,4},{6,7},{7,6},{8,9},{9,8},{10,11... | collective-permute-start | bytes 786440 | tf_op jit(solution)/shard_map/ppermute | solution.py:67
  64.4 7.5 %collective-permute-start.33 = (bf16[48,1024]{1,0:T(8,128)(2,1)S(1)}, bf16[48,1024]{1,0:T(8,128)(2,1)S(1)}, u32[]{:S(2)}, u32[]{:S(2)}) collective-permute-start(bf16[48,1024]{1,0:T(8,128)(2,1)S(1)} %shard_map.241.refs_0_), channel_id=1, source_target_pairs={{0,2},{1,3},{2,0},{3,1},{4,6},{5,7},{6,4},{7,5},{8,10},{9,11},{10,... | collective-permute-start | bytes 294920 | tf_op jit(solution)/shard_map/ppermute | solution.py:52
  68.7 9.6 %collective-permute-start.34 = (bf16[48,1024]{1,0:T(8,128)(2,1)S(1)}, bf16[48,1024]{1,0:T(8,128)(2,1)S(1)}, u32[]{:S(2)}, u32[]{:S(2)}) collective-permute-start(bf16[48,1024]{1,0:T(8,128)(2,1)S(1)} %shard_map.241.refs_0_), channel_id=1, source_target_pairs={{0,4},{1,5},{2,6},{3,7},{4,0},{5,1},{6,2},{7,3},{8,12},{9,13},{10,... | collective-permute-start | bytes 294920 | tf_op jit(solution)/shard_map/ppermute | solution.py:52
  69.1 9.3 %collective-permute-start.35 = (bf16[48,1024]{1,0:T(8,128)(2,1)S(1)}, bf16[48,1024]{1,0:T(8,128)(2,1)S(1)}, u32[]{:S(2)}, u32[]{:S(2)}) collective-permute-start(bf16[48,1024]{1,0:T(8,128)(2,1)S(1)} %shard_map.241.refs_0_), channel_id=1, source_target_pairs={{0,6},{1,7},{2,4},{3,5},{4,2},{5,3},{6,0},{7,1},{8,14},{9,15},{10,... | collective-permute-start | bytes 294920 | tf_op jit(solution)/shard_map/ppermute | solution.py:52
  71.2 11.9 %collective-permute-start.36 = (bf16[48,1024]{1,0:T(8,128)(2,1)S(1)}, bf16[48,1024]{1,0:T(8,128)(2,1)S(1)}, u32[]{:S(2)}, u32[]{:S(2)}) collective-permute-start(bf16[48,1024]{1,0:T(8,128)(2,1)S(1)} %shard_map.241.refs_0_), channel_id=1, source_target_pairs={{0,1},{1,0},{2,3},{3,2},{4,5},{5,4},{6,7},{7,6},{8,9},{9,8},{10,11... | collective-permute-start | bytes 294920 | tf_op jit(solution)/shard_map/ppermute | solution.py:74
  71.9 12.3 %collective-permute-start.37 = (bf16[48,1024]{1,0:T(8,128)(2,1)S(1)}, bf16[48,1024]{1,0:T(8,128)(2,1)S(1)}, u32[]{:S(2)}, u32[]{:S(2)}) collective-permute-start(bf16[48,1024]{1,0:T(8,128)(2,1)S(1)} %collective-permute-done.33.refs_1_), channel_id=1, source_target_pairs={{0,1},{1,0},{2,3},{3,2},{4,5},{5,4},{6,7},{7,6},{8,9},{9,8},{10,11... | collective-permute-start | bytes 294920 | tf_op jit(solution)/shard_map/ppermute | solution.py:74
  78.4 7.3 %collective-permute-start.38 = (bf16[48,1024]{1,0:T(8,128)(2,1)S(1)}, bf16[48,1024]{1,0:T(8,128)(2,1)S(1)}, u32[]{:S(2)}, u32[]{:S(2)}) collective-permute-start(bf16[48,1024]{1,0:T(8,128)(2,1)S(1)} %collective-permute-done.34.refs_2_), channel_id=1, source_target_pairs={{0,1},{1,0},{2,3},{3,2},{4,5},{5,4},{6,7},{7,6},{8,9},{9,8},{10,11... | collective-permute-start | bytes 294920 | tf_op jit(solution)/shard_map/ppermute | solution.py:74
  78.4 7.3 %collective-permute-start.39 = (bf16[48,1024]{1,0:T(8,128)(2,1)S(1)}, bf16[48,1024]{1,0:T(8,128)(2,1)S(1)}, u32[]{:S(2)}, u32[]{:S(2)}) collective-permute-start(bf16[48,1024]{1,0:T(8,128)(2,1)S(1)} %collective-permute-done.35.refs_3_), channel_id=1, source_target_pairs={{0,1},{1,0},{2,3},{3,2},{4,5},{5,4},{6,7},{7,6},{8,9},{9,8},{10,11... | collective-permute-start | bytes 294920 | tf_op jit(solution)/shard_map/ppermute | solution.py:74
  78.9 11.1 %collective-permute-start.25 = (bf16[64,512]{1,0:T(8,128)(2,1)S(1)}, bf16[64,512]{1,0:T(8,128)(2,1)S(1)}, u32[]{:S(2)}, u32[]{:S(2)}) collective-permute-start(bf16[64,512]{1,0:T(8,128)(2,1)S(1)} %get-tuple-element.59), channel_id=1, source_target_pairs={{0,6},{1,7},{2,4},{3,5},{4,2},{5,3},{6,0},{7,1},{8,14},{9,15},{10,... | collective-permute-start | bytes 196616 | tf_op jit(solution)/shard_map/ppermute | solution.py:52
  83.1 8.4 %collective-permute-start.24 = (bf16[64,512]{1,0:T(8,128)(2,1)S(1)}, bf16[64,512]{1,0:T(8,128)(2,1)S(1)}, u32[]{:S(2)}, u32[]{:S(2)}) collective-permute-start(bf16[64,512]{1,0:T(8,128)(2,1)S(1)} %get-tuple-element.60), channel_id=1, source_target_pairs={{0,4},{1,5},{2,6},{3,7},{4,0},{5,1},{6,2},{7,3},{8,12},{9,13},{10,... | collective-permute-start | bytes 196616 | tf_op jit(solution)/shard_map/ppermute | solution.py:52
  84.2 7.4 %collective-permute-start.23 = (bf16[64,512]{1,0:T(8,128)(2,1)S(1)}, bf16[64,512]{1,0:T(8,128)(2,1)S(1)}, u32[]{:S(2)}, u32[]{:S(2)}) collective-permute-start(bf16[64,512]{1,0:T(8,128)(2,1)S(1)} %get-tuple-element.58), channel_id=1, source_target_pairs={{0,2},{1,3},{2,0},{3,1},{4,6},{5,7},{6,4},{7,5},{8,10},{9,11},{10,... | collective-permute-start | bytes 196616 | tf_op jit(solution)/shard_map/ppermute | solution.py:52
  (11 other events, 73.9 us)
